TPU v7x, 128 devices: a whole 4x4x4 slice. The times are simulated.
128 devices in a mesh: sp: 32 (over z, y, core), tp: 4 (over x).
Axes of the slice: x: 4, y: 4, z: 4, core: 2. Of those that a mesh axis runs over, the one named last changes fastest.
Arguments:
- queries: bfloat16 [32768, 1024], P('sp', 'tp'), may hold values from -8 to 8
- keys: bfloat16 [32768, 256], P('sp', 'tp'), may hold values from -8 to 8
- values: bfloat16 [32768, 256], P('sp', 'tp'), may hold values from -18 to 18
- doc_ids: int32 [32768], P('sp'), may hold values from 0 to 7, never falling along the last dimension, each value on 1 to 16384 neighbouring positions
- sinks: float32 [16], P('tp'), may hold values from 0 to 4
- residual: bfloat16 [32768, 2048], P(('sp', 'tp')), may hold values from -12 to 12
- out_weight: bfloat16 [1024, 2048], P('tp'), may hold values from -0.1875 to 0.1875
- norm_gain: float32 [2048], replicated, may hold values from 0.1 to 1.9
- w_gate: bfloat16 [2048, 5632], P('sp', 'tp'), may hold values from -0.125 to 0.125
- w_value: bfloat16 [2048, 5632], P('sp', 'tp'), may hold values from -0.125 to 0.125
- conv_gate: float32 [3, 5632], P(None, 'tp'), may hold values from -3.5 to 3.5
- conv_value: float32 [3, 5632], P(None, 'tp'), may hold values from -3.5 to 3.5
- w_down: bfloat16 [5632, 2048], P('tp', 'sp'), may hold values from -0.078125 to 0.078125
Outputs:
- layer_out: bfloat16 [32768, 2048], P(('sp', 'tp'))
All inputs are finite; a program needn't handle non-finite values.
Results may differ from a plain program's by a relative error of at most 0.012.
Values may be sent and summed in bfloat16 or wider, within the bound.
A program may use at most 128 MiB of HBM per device.

v0:
```python
import jax
import jax.numpy as jnp
from jax import lax
from jax.sharding import PartitionSpec as P

HEAD_DIM = 64
WINDOW = 128


def shifted(shard, axis, by):
    size = lax.axis_size(axis)
    pairs = [(i, i + by) for i in range(size) if 0 <= i + by < size]
    return lax.ppermute(shard, axis, pairs)


def joined_along(pieces, dim):
    shape = list(pieces.shape[1:])
    shape[dim] *= pieces.shape[0]
    return jnp.moveaxis(pieces, 0, dim).reshape(shape)


def sent_to_all(shard, axis):
    size = lax.axis_size(axis)
    return lax.all_to_all(
        jnp.broadcast_to(shard[None], (size, *shard.shape)), axis, 0, 0, tiled=True
    )


def gathered_copies(shard, axis, dim):
    return joined_along(sent_to_all(shard, axis), dim)


def side_by_side(arrays, axis, dim, along):
    both = jnp.concatenate(arrays, axis=along)
    out, at, done = (lax.all_gather(both, axis, axis=dim, tiled=True), 0, [])
    for a in arrays:
        done.append(lax.slice_in_dim(out, at, at + a.shape[along], axis=along))
        at += a.shape[along]
    return tuple(done)


def attend(query_rows, key_ext, value_ext, doc_rows, doc_ext, sinks):
    row_count = query_rows.shape[0]
    block_count = row_count // WINDOW
    kv_heads = key_ext.shape[1] // HEAD_DIM
    group_size = query_rows.shape[1] // (kv_heads * HEAD_DIM)

    def band(t):
        lower = t[:row_count].reshape((block_count, WINDOW) + t.shape[1:])
        upper = t[WINDOW:].reshape((block_count, WINDOW) + t.shape[1:])
        return jnp.concatenate([lower, upper], axis=1)

    query_band = query_rows.reshape(block_count, WINDOW, kv_heads, group_size, HEAD_DIM)
    key_band = band(key_ext).reshape(block_count, 2 * WINDOW, kv_heads, HEAD_DIM)
    value_band = band(value_ext).reshape(block_count, 2 * WINDOW, kv_heads, HEAD_DIM)
    doc_band = band(doc_ext)
    distance = jnp.arange(WINDOW)[:, None] + WINDOW - jnp.arange(2 * WINDOW)[None, :]
    in_window = (distance >= 0) & (distance < WINDOW)
    same_doc = doc_rows.reshape(block_count, WINDOW)[:, :, None] == doc_band[:, None, :]
    keep_mask = in_window[None] & same_doc
    scores = jnp.einsum(
        "nqhgd,nkhd->nhgqk", query_band, key_band, preferred_element_type=jnp.float32
    ) * HEAD_DIM ** (-0.5)
    scores = jnp.where(keep_mask[:, None, None], scores, -jnp.inf)
    sink_logit = sinks.reshape(kv_heads, group_size)[None, :, :, None, None]
    peak = jnp.maximum(jnp.max(scores, axis=-1, keepdims=True), sink_logit)
    expd = jnp.exp(scores - peak)
    probs = (expd / (jnp.sum(expd, axis=-1, keepdims=True) + jnp.exp(sink_logit - peak))).astype(
        jnp.bfloat16
    )
    mixed = jnp.einsum("nhgqk,nkhd->nqhgd", probs, value_band, preferred_element_type=jnp.float32)
    return mixed.astype(jnp.bfloat16).reshape(row_count, -1)


def convolve(ext_rows, doc_ext, taps):
    center = doc_ext[2:]
    same_one = (doc_ext[1:-1] == center)[:, None]
    same_two = (doc_ext[:-2] == center)[:, None]
    ext32 = ext_rows.astype(jnp.float32)
    result = taps[2] * ext32[2:]
    result = result + jnp.where(same_one, taps[1] * ext32[1:-1], 0.0)
    return result + jnp.where(same_two, taps[0] * ext32[:-2], 0.0)


def per_device(
    queries,
    keys,
    values,
    doc_ids,
    sinks,
    residual,
    out_weight,
    norm_gain,
    w_gate,
    w_value,
    conv_gate,
    conv_value,
    w_down,
):
    docs_plus = doc_ids + 1
    prev_keys, prev_values, prev_docs = shifted(
        (keys[-WINDOW:], values[-WINDOW:], docs_plus[-WINDOW:]), "sp", 1
    )
    key_ext = jnp.concatenate([prev_keys, keys], axis=0)
    value_ext = jnp.concatenate([prev_values, values], axis=0)
    doc_ext = jnp.concatenate([prev_docs, docs_plus], axis=0)
    head_out = attend(queries, key_ext, value_ext, docs_plus, doc_ext, sinks)
    head_rows = lax.all_to_all(head_out, "tp", split_axis=0, concat_axis=1, tiled=True)
    proj = jnp.dot(
        head_rows,
        lax.all_gather(out_weight, "tp", axis=0, tiled=True),
        preferred_element_type=jnp.float32,
    )
    mid32 = (residual.astype(jnp.float32) + proj).astype(jnp.bfloat16).astype(jnp.float32)
    normed = (
        mid32 * lax.rsqrt(jnp.mean(mid32 * mid32, axis=-1, keepdims=True) + 1e-06) * norm_gain
    ).astype(jnp.bfloat16)
    whole = gathered_copies(normed, "tp", 0)

    def add_rows(piece):
        return jnp.dot(whole, piece, preferred_element_type=jnp.float32)

    pieces = side_by_side((w_gate, w_value), "sp", 0, 1)
    gate_sum = add_rows(pieces[0])
    value_sum = add_rows(pieces[1])
    gate_pre = gate_sum.astype(jnp.bfloat16)
    value_pre = value_sum.astype(jnp.bfloat16)
    prev_gate, prev_value = shifted((gate_pre[-2:], value_pre[-2:]), "sp", 1)
    conv_docs = jnp.concatenate([prev_docs[-2:], docs_plus], axis=0)
    gate_conv = convolve(jnp.concatenate([prev_gate, gate_pre], axis=0), conv_docs, conv_gate)
    value_conv = convolve(jnp.concatenate([prev_value, value_pre], axis=0), conv_docs, conv_value)
    hidden = (jax.nn.silu(gate_conv) * value_conv).astype(jnp.bfloat16)
    terms = jnp.dot(
        hidden, lax.all_gather(w_down, "sp", axis=1, tiled=True), preferred_element_type=jnp.float32
    )
    sums = lax.psum_scatter(
        terms.astype(jnp.bfloat16), "tp", scatter_dimension=0, tiled=True
    ).astype(jnp.float32)
    return (mid32 + sums).astype(jnp.bfloat16)


def solution(mesh):
    return jax.shard_map(
        per_device,
        mesh=mesh,
        in_specs=(
            P("sp", "tp"),
            P("sp", "tp"),
            P("sp", "tp"),
            P("sp"),
            P("tp"),
            P(("sp", "tp"), None),
            P("tp", None),
            P(),
            P("sp", "tp"),
            P("sp", "tp"),
            P(None, "tp"),
            P(None, "tp"),
            P("tp", "sp"),
        ),
        out_specs=P(("sp", "tp"), None),
        check_vma=False,
    )
```

profile of v0, /device:TPU:1, one launch (start us, length us, event | category | flops | bytes accessed | tf_op | source)
XLA Modules:
  0.0 256.3 jit_solution(1870494783780439739)
XLA Ops:
  7.3 1.8 pad_maximum_fusion
  9.8 4.6 %collective-permute-start.1 = (s32[128]{0:T(128)S(1)}, s32[128]{0:T(128)S(1)}, u32[]{:S(2)}, u32[]{:S(2)}) collective-permute-start(s32[128]{0:T(128)S(1)} %slice.89), channel_id=1, source_target_pairs={{0,4},{4,8},{8,12},{12,16},{16,20},{20,24},{24,28},{28,32},{32,36}... | collective-permute-start | bytes 1544 | tf_op jit(solution)/shard_map/ppermute | solution.py:13
  15.2 1.9 collective-permute-start.2
  17.8 3.6 %collective-permute-start = (bf16[128,64]{0,1:T(8,128)(2,1)S(1)}, bf16[128,64]{0,1:T(8,128)(2,1)S(1)}, u32[]{:S(2)}, u32[]{:S(2)}) collective-permute-start(bf16[128,64]{0,1:T(8,128)(2,1)S(1)} %slice.87), channel_id=1, source_target_pairs={{0,4},{4,8},{8,12},{12,16},{16,20},{20,24},{24,28},{28,32},{32,36}... | collective-permute-start | bytes 49160 | tf_op jit(solution)/shard_map/ppermute | solution.py:13
  23.4 2.1 reshape.131
  26.9 1.0 fusion.20
  28.0 1.2 fusion.34
  30.0 19.1 %all_to_all.24 = bf16[4,256,256]{1,2,0:T(8,128)(2,1)S(1)} all-to-all(bf16[4,256,256]{1,2,0:T(8,128)(2,1)S(1)} %copy.33), channel_id=1, replica_groups=mesh['sp'=32,'tp'=4] {'tp'}, dimensions={0} | all-to-all | bytes 1048576 | tf_op jit(solution)/shard_map/all_to_all | solution.py:108
  49.1 16.7 %all-gather.4.cloned.1.call-done = bf16[1024,2048]{1,0:T(8,128)(2,1)} async-done(((bf16[256,2048]{1,0:T(8,128)(2,1)}), bf16[1024,2048]{1,0:T(8,128)(2,1)}) %all-gather.4.cloned.1.call-update) | async-done | bytes 4194320 | tf_op jit(solution)/shard_map/all_gather | solution.py:111
  65.8 3.6 %fusion.24 = (f32[256]{0:T(256)S(1)}, bf16[256,2048]{1,0:T(8,128)(2,1)S(1)}) fusion(bf16[256,1024]{0,1:T(8,128)(2,1)S(1)} %bitcast.77, bf16[1024,2048]{1,0:T(8,128)(2,1)} %all-gather.4.cloned.1.call-done, bf16[256,2048]{1,0:T(8,128)(2,1)S(1)} %copy-done.7), kind=kOutput, calls=%fused_computation.35 | convolution fusion | flops 1076887296 | bytes 6816768 | tf_op jit(solution)/shard_map/dot_general | solution.py:109
  69.8 2.6 broadcast_in_dim.59
  72.3 5.0 %all-to-all-start.1 = ((bf16[4,256,2048]{2,1,0:T(8,128)(2,1)}), bf16[4,256,2048]{2,1,0:T(8,128)(2,1)}, u32[]{:S(2)}, u32[]{:S(2)}) async-start(bf16[4,256,2048]{2,1,0:T(8,128)(2,1)} %broadcast_in_dim.59), calls=%async_computation.1 | async-start | bytes 8388608 | tf_op jit(solution)/shard_map/all_to_all | solution.py:24
  77.7 47.8 %all-to-all-done.1 = bf16[4,256,2048]{2,1,0:T(8,128)(2,1)} async-done(((bf16[4,256,2048]{2,1,0:T(8,128)(2,1)}), bf16[4,256,2048]{2,1,0:T(8,128)(2,1)}, u32[]{:S(2)}, u32[]{:S(2)}) %all-to-all-start.1) | async-done | bytes 4194336 | tf_op jit(solution)/shard_map/all_to_all | solution.py:24
  125.5 3.9 %all-gather.6.cloned.1.call-done = bf16[2048,2816]{1,0:T(8,128)(2,1)} async-done(((bf16[64,2816]{1,0:T(8,128)(2,1)}), bf16[2048,2816]{1,0:T(8,128)(2,1)}) %all-gather.6.cloned.1.call-update) | async-done | bytes 11534352 | tf_op jit(solution)/shard_map/all_gather | solution.py:35
  129.3 10.3 %fusion.14 = bf16[1024,1408]{1,0:T(8,128)(2,1)S(1)} fusion(bf16[1024,2048]{1,0:T(8,128)(2,1)} %bitcast.13, bf16[2048,2816]{1,0:T(8,128)(2,1)} %all-gather.6.cloned.1.call-done), kind=kOutput, calls=%fused_computation.23 | convolution fusion | flops 5907021824 | bytes 12845056 | tf_op jit(solution)/shard_map/dot_general | solution.py:121
  139.6 3.4 %collective-permute-start.3 = (bf16[2,1408]{1,0:T(2,128)(2,1)S(1)}, bf16[2,1408]{1,0:T(2,128)(2,1)S(1)}, u32[]{:S(2)}, u32[]{:S(2)}) collective-permute-start(bf16[2,1408]{1,0:T(2,128)(2,1)S(1)} %slice.114), channel_id=1, source_target_pairs={{0,4},{4,8},{8,12},{12,16},{16,20},{20,24},{24,28},{28,32},{32,36}... | collective-permute-start | bytes 16904 | tf_op jit(solution)/shard_map/ppermute | solution.py:13
  143.1 8.5 %fusion.17 = bf16[1024,1408]{1,0:T(8,128)(2,1)S(1)} fusion(bf16[1024,2048]{1,0:T(8,128)(2,1)} %bitcast.13, bf16[2048,2816]{1,0:T(8,128)(2,1)S(1)} %copy-done.6), kind=kOutput, calls=%fused_computation.24 | convolution fusion | flops 5907021824 | bytes 12845056 | tf_op jit(solution)/shard_map/dot_general | solution.py:121
  151.6 2.2 collective-permute-start.4
  153.8 3.0 %maximum_convert_fusion = f32[1026,1408]{1,0:T(8,128)} fusion(bf16[1024,1408]{1,0:T(8,128)(2,1)S(1)} %fusion.14, bf16[2,1408]{1,0:T(2,128)(2,1)S(1)} %collective-permute-done.3), kind=kLoop, calls=%fused_computation.31 | loop fusion | flops 5778432 | bytes 8667648 | tf_op jit(solution)/shard_map/convert_element_type | solution.py:79
  156.8 3.1 %maximum_convert_fusion.1 = f32[1026,1408]{1,0:T(8,128)} fusion(bf16[1024,1408]{1,0:T(8,128)(2,1)S(1)} %fusion.17, bf16[2,1408]{1,0:T(2,128)(2,1)S(1)} %collective-permute-done.4), kind=kLoop, calls=%fused_computation.32 | loop fusion | flops 5778432 | bytes 8667648 | tf_op jit(solution)/shard_map/convert_element_type | solution.py:79
  159.9 19.4 %all-gather.8.cloned.1.call-done = bf16[1408,2048]{0,1:T(8,128)(2,1)} async-done(((bf16[1408,64]{0,1:T(8,128)(2,1)}), bf16[1408,2048]{0,1:T(8,128)(2,1)}) %all-gather.8.cloned.1.call-update) | async-done | bytes 5767184 | tf_op jit(solution)/shard_map/all_gather | solution.py:134
  179.3 22.3 %convolution_convert_fusion = bf16[1024,2048]{1,0:T(8,128)(2,1)} fusion(bf16[1408,2048]{0,1:T(8,128)(2,1)} %all-gather.8.cloned.1.call-done, f32[1026,1408]{1,0:T(8,128)} %maximum_convert_fusion.1, f32[1026,1408]{1,0:T(8,128)} %maximum_convert_fusion, f32[1408]{0:T(1024)S(1)} %get-tuple-element.9, f32[1408]{0:T(1024)S(1)} %get-tuple-element.10, ...), kind=kOutput, calls=%fused_computation.25 | convolution fusion | flops 5936513024 | bytes 44600320 | tf_op jit(solution)/shard_map/dot_general | solution.py:133
  201.7 45.4 %reduce-scatter.2.cloned.1.call-done = bf16[256,2048]{1,0:T(8,128)(2,1)} async-done(((bf16[1024,2048]{1,0:T(8,128)(2,1)}), bf16[256,2048]{1,0:T(8,128)(2,1)}) %reduce-scatter.2.cloned.1.call-update) | async-done | bytes 1048592 | tf_op jit(solution)/shard_map/reduce_scatter | solution.py:136
  247.1 2.6 %fusion.27 = bf16[256,2048]{1,0:T(8,128)(2,1)} fusion(bf16[256,2048]{1,0:T(8,128)(2,1)S(1)} %get-tuple-element.18, bf16[256,2048]{1,0:T(8,128)(2,1)} %reduce-scatter.2.cloned.1.call-done), kind=kLoop, calls=%fused_computation.38 | loop fusion | flops 2097152 | bytes 3145728 | tf_op jit(solution)/shard_map/convert_element_type | solution.py:139
  (55 shorter events, 7.8 us)
Async XLA Ops:
  6.5 19.3 %copy-start = (bf16[1024,64]{0,1:T(8,128)(2,1)S(1)}, bf16[1024,64]{0,1:T(8,128)(2,1)}, u32[]{:S(2)}) copy-start(bf16[1024,64]{0,1:T(8,128)(2,1)} %param.14) | copy-start | bytes 393220
  6.5 59.3 %all-gather.4.cloned.1.call-start = ((), (), s32[]{:S(2)}) async-start(), calls=%async_computation.3 | async-start | bytes 5242880 | tf_op jit(solution)/shard_map/all_gather | solution.py:111
  7.3 122.1 %all-gather.6.cloned.1.call-start = ((), (), s32[]{:S(2)}) async-start(), calls=%async_computation.4 | async-start | bytes 11894784 | tf_op jit(solution)/shard_map/all_gather | solution.py:35
  9.1 170.2 %all-gather.8.cloned.1.call-start = ((), (), s32[]{:S(2)}) async-start(), calls=%async_computation.5 | async-start | bytes 5947392 | tf_op jit(solution)/shard_map/all_gather | solution.py:134
  9.8 15.6 %collective-permute-start.1 = (s32[128]{0:T(128)S(1)}, s32[128]{0:T(128)S(1)}, u32[]{:S(2)}, u32[]{:S(2)}) collective-permute-start(s32[128]{0:T(128)S(1)} %slice.89), channel_id=1, source_target_pairs={{0,4},{4,8},{8,12},{12,16},{16,20},{20,24},{24,28},{28,32},{32,36}... | collective-permute-start | bytes 1544 | tf_op jit(solution)/shard_map/ppermute | solution.py:13
  15.2 10.7 %collective-permute-start.2 = (bf16[128,64]{0,1:T(8,128)(2,1)S(1)}, bf16[128,64]{0,1:T(8,128)(2,1)S(1)}, u32[]{:S(2)}, u32[]{:S(2)}) collective-permute-start(bf16[128,64]{0,1:T(8,128)(2,1)S(1)} %slice.92), channel_id=1, source_target_pairs={{0,4},{4,8},{8,12},{12,16},{16,20},{20,24},{24,28},{28,32},{32,36}... | collective-permute-start | bytes 49160 | tf_op jit(solution)/shard_map/ppermute | solution.py:13
  17.8 10.2 %collective-permute-start = (bf16[128,64]{0,1:T(8,128)(2,1)S(1)}, bf16[128,64]{0,1:T(8,128)(2,1)S(1)}, u32[]{:S(2)}, u32[]{:S(2)}) collective-permute-start(bf16[128,64]{0,1:T(8,128)(2,1)S(1)} %slice.87), channel_id=1, source_target_pairs={{0,4},{4,8},{8,12},{12,16},{16,20},{20,24},{24,28},{28,32},{32,36}... | collective-permute-start | bytes 49160 | tf_op jit(solution)/shard_map/ppermute | solution.py:13
  22.4 4.5 %copy-start.5 = (f32[4]{0:T(128)S(1)}, f32[4]{0:T(128)}, u32[]{:S(2)}) copy-start(f32[4]{0:T(128)} %param.17) | copy-start | bytes 52
  25.9 2.1 copy-start.1
  29.2 36.6 %copy-start.7 = (bf16[256,2048]{1,0:T(8,128)(2,1)S(1)}, bf16[256,2048]{1,0:T(8,128)(2,1)}, u32[]{:S(2)}) copy-start(bf16[256,2048]{1,0:T(8,128)(2,1)} %param.18) | copy-start | bytes 3145732
  49.1 20.3 %copy-start.4 = (f32[2048]{0:T(1024)S(1)}, f32[2048]{0:T(1024)}, u32[]{:S(2)}) copy-start(f32[2048]{0:T(1024)} %param.20) | copy-start | bytes 24580
  72.3 5.0 %copy-start.2 = (f32[3,1408]{1,0:T(4,128)S(1)}, f32[3,1408]{1,0:T(4,128)}, u32[]{:S(2)}) copy-start(f32[3,1408]{1,0:T(4,128)} %param.24) | copy-start | bytes 50692
  72.3 5.1 %copy-start.3 = (f32[3,1408]{1,0:T(4,128)S(1)}, f32[3,1408]{1,0:T(4,128)}, u32[]{:S(2)}) copy-start(f32[3,1408]{1,0:T(4,128)} %param.23) | copy-start | bytes 50692
  72.3 53.1 %all-to-all-start.1 = ((bf16[4,256,2048]{2,1,0:T(8,128)(2,1)}), bf16[4,256,2048]{2,1,0:T(8,128)(2,1)}, u32[]{:S(2)}, u32[]{:S(2)}) async-start(bf16[4,256,2048]{2,1,0:T(8,128)(2,1)} %broadcast_in_dim.59), calls=%async_computation.1 | async-start | bytes 8388608 | tf_op jit(solution)/shard_map/all_to_all | solution.py:24
  77.3 169.8 %reduce-scatter.2.cloned.1.call-start = ((), (), s32[]{:S(2)}) async-start(), calls=%async_computation.6 | async-start | bytes 5242880 | tf_op jit(solution)/shard_map/reduce_scatter | solution.py:136
  129.3 13.7 %copy-start.6 = (bf16[2048,2816]{1,0:T(8,128)(2,1)S(1)}, bf16[2048,2816]{1,0:T(8,128)(2,1)}, u32[]{:S(2)}) copy-start(bf16[2048,2816]{1,0:T(8,128)(2,1)} %all-gather.6.cloned.1.call-done) | copy-start | bytes 34603012
  139.6 14.1 %collective-permute-start.3 = (bf16[2,1408]{1,0:T(2,128)(2,1)S(1)}, bf16[2,1408]{1,0:T(2,128)(2,1)S(1)}, u32[]{:S(2)}, u32[]{:S(2)}) collective-permute-start(bf16[2,1408]{1,0:T(2,128)(2,1)S(1)} %slice.114), channel_id=1, source_target_pairs={{0,4},{4,8},{8,12},{12,16},{16,20},{20,24},{24,28},{28,32},{32,36}... | collective-permute-start | bytes 16904 | tf_op jit(solution)/shard_map/ppermute | solution.py:13
  151.6 5.2 %collective-permute-start.4 = (bf16[2,1408]{1,0:T(2,128)(2,1)S(1)}, bf16[2,1408]{1,0:T(2,128)(2,1)S(1)}, u32[]{:S(2)}, u32[]{:S(2)}) collective-permute-start(bf16[2,1408]{1,0:T(2,128)(2,1)S(1)} %slice.121), channel_id=1, source_target_pairs={{0,4},{4,8},{8,12},{12,16},{16,20},{20,24},{24,28},{28,32},{32,36}... | collective-permute-start | bytes 16904 | tf_op jit(solution)/shard_map/ppermute | solution.py:13
Sparse Core Ops, SparseCore 0:
  9.0 56.8 all-gather.3
  68.1 61.1 all-gather.5
  131.6 47.7 all-gather.7
  201.8 45.2 reduce-scatter.1
where the time goes:
time: 257 us; the launch traced here: 256 us
  waiting for transfers between devices  134 us (52%)
  matrix products  46.8 us (18%)
  starting transfers between devices  20.8 us (8%)
  blocking collectives  19.1 us (7%)
  between operations  13.4 us (5%)
  other arithmetic  13.2 us (5%)
  local copies, waits for them, and re-layouts  8.96 us (3%)
    all_to_all x1, waiting for transfers between devices, sent_to_all(): lax.all_to_all(jnp.broadcast_to(shard[None], (size, *shard.shape)), axis,...  47.8 us
    reduce_scatter x1, waiting for transfers between devices, per_device(): lax.psum_scatter(terms.astype(jnp.bfloat16), 'tp', scatter_dimension=0, t...  45.4 us
    dot_general x1, matrix products, per_device(): jnp.dot(hidden, lax.all_gather(w_down, 'sp', axis=1, tiled=True), preferr...  22.3 us
    all_gather x1, waiting for transfers between devices, per_device(): lax.all_gather(w_down, 'sp', axis=1, tiled=True)  19.4 us
    all_to_all x1, blocking collectives, per_device(): lax.all_to_all(head_out, 'tp', split_axis=0, concat_axis=1, tiled=True)  19.1 us
    dot_general x2, matrix products, add_rows(): return jnp.dot(whole, piece, preferred_element_type=jnp.float32)  18.7 us
    all_gather x1, waiting for transfers between devices, per_device(): lax.all_gather(out_weight, 'tp', axis=0, tiled=True)  16.7 us
    ppermute x5, starting transfers between devices, shifted(): return lax.ppermute(shard, axis, pairs)  15.7 us
  transfers between devices with their start and end apart: 10, of which 5 were waited for; matrix products, arithmetic and copies ran while one was open for 17% of the time, Pallas kernels for 0%

commit v1 on v0

v1 whole, which is shorter than its diff:
```python
import functools

import jax
import jax.numpy as jnp
from jax import lax
from jax.experimental import pallas as pl
from jax.experimental.pallas import tpu as pltpu
from jax.sharding import PartitionSpec as P

HEAD_DIM = 64
WINDOW = 128
MESH = pl.DeviceIdType.MESH
F32 = jnp.float32
BF16 = jnp.bfloat16
NT = (((1,), (1,)), ((), ()))

N_SP = 32
ROWS = 1024
BLK = 256
D = 2048
HID = 1408
HALO = 16
EXT = BLK + HALO
N_SEM = 256


def ceil_dot(a, b):
    return jnp.dot(a, b, preferred_element_type=F32)


def nt_dot(a, b):
    return lax.dot_general(a, b, NT, preferred_element_type=F32)


def kernel(
    q_in,
    kv_in,
    drow_in,
    dcol_in,
    sinks,
    res_in,
    ow_in,
    gain_in,
    wg_in,
    wv_in,
    cg_in,
    cv_in,
    wd_in,
    out,
    q,
    kv,
    kvz,
    drow,
    dcol,
    m1,
    m2,
    att,
    af,
    ow,
    res,
    mid,
    gain,
    nb,
    wu,
    wd,
    pre,
    hid,
    cg,
    cv,
    own,
    pr,
    prf,
    pl_,
    plf,
    pf,
    rl,
    rr,
    tl,
    tr,
    send_sem,
    recv_sem,
    loc_sem,
):
    sp = lax.axis_index("sp")
    x = lax.axis_index("tp")
    c = lax.rem(sp, 2)
    k = lax.div(sp, 2)
    y = lax.rem(k, 4)
    z = lax.div(k, 4)

    def sp_of(zz, yy):
        return (lax.rem(zz + 8, 4) * 4 + lax.rem(yy + 8, 4)) * 2 + c

    def xat(j):
        return lax.rem(x + j + 4, 4)

    def dev(s, t):
        return {"sp": s, "tp": t}

    sp_next = lax.rem(sp + 1, N_SP)
    sp_prev = lax.rem(sp + N_SP - 1, N_SP)
    sib = sp + 1 - 2 * c

    loc = []

    def local(src, dst):
        cp = pltpu.make_async_copy(src, dst, loc_sem.at[len(loc)])
        cp.start()
        loc.append(cp)
        return cp

    piece = (pl.ds(pl.multiple_of(k * 16, 16), 16), pl.ds(pl.multiple_of(c * 1024, 1024), 1024))
    l_kv = local(kv_in, kv.at[pl.ds(WINDOW, ROWS)])
    l_drow = local(drow_in, drow.at[pl.ds(8, 8)])
    l_dcol = local(dcol_in, dcol.at[pl.ds(HALO, ROWS)])
    l_ow = local(ow_in.at[piece], ow.at[x, k, :, piece[1]])
    row64 = pl.ds(pl.multiple_of(sp * 64, 64), 64)
    l_wg = local(wg_in, wu.at[row64, pl.ds(0, HID)])
    l_wv = local(wv_in, wu.at[row64, pl.ds(HID, HID)])
    l_wd = local(wd_in, wd.at[row64])
    l_q = local(q_in, q)
    l_res = local(res_in, res)
    l_gain = local(gain_in, gain)
    l_cg = local(cg_in, cg)
    l_cv = local(cv_in, cv)

    bar = pltpu.get_barrier_semaphore()

    def hello(d):
        pl.semaphore_signal(bar, inc=1, device_id=d, device_id_type=MESH)

    for j in (1, 2, 3):
        hello(dev(sp, xat(j)))
    for dz, dy in ((0, 1), (0, -1), (1, 0), (-1, 0)):
        hello(dev(sp_of(z + dz, y + dy), x))
    hello(dev(sib, x))
    for j in range(4):
        hello(dev(sp_prev, xat(j)))
    pl.semaphore_wait(bar, 12)

    copies = []

    def push(src, dst, d):
        i = len(copies)
        cp = pltpu.make_async_remote_copy(
            src_ref=src,
            dst_ref=dst,
            send_sem=send_sem.at[i],
            recv_sem=recv_sem.at[i],
            device_id=d,
            device_id_type=MESH,
        )
        cp.start()
        copies.append(cp)
        return cp

    l_kv.wait()
    l_drow.wait()
    l_dcol.wait()
    nxt = dev(sp_next, x)
    h_kv = push(kv.at[pl.ds(ROWS, WINDOW)], kv.at[pl.ds(0, WINDOW)], nxt)
    h_drow = push(drow.at[pl.ds(8, 8)], drow.at[pl.ds(0, 8)], nxt)
    h_dcol = push(dcol.at[pl.ds(ROWS, HALO)], dcol.at[pl.ds(0, HALO)], nxt)

    l_ow.wait()
    ow_x = [
        push(ow.at[x, k, :, piece[1]], ow.at[x, k, :, piece[1]], dev(sp, xat(j)))
        for j in (1, 3, 2)
    ]

    def ow_view(half, kk, cc, part):
        col = pl.ds(pl.multiple_of(cc * 1024, 1024), 1024)
        if part is None:
            return ow.at[pl.ds(2 * half, 2), kk, :, col]
        return ow.at[2 * half + part, kk, :, col]

    def wu_view(half, kk, cc, part):
        r = (kk * 2 + cc) * 64
        n = 64 if part is None else 32
        if part == 1:
            r = r + 32
        return wu.at[pl.ds(pl.multiple_of(r, 32), n), pl.ds(half * HID, HID)]

    def wd_view(half, kk, cc, part):
        r = (kk * 2 + cc) * 64 + 32 * half
        n = 32 if part is None else 16
        if part == 1:
            r = r + 16
        return wd.at[pl.ds(pl.multiple_of(r, 16), n)]

    class Gather:
        def __init__(self, view):
            self.view = view
            self.sibs = []
            self.h = [{}, {}]

        def at(self, half, dp, dq, part=None):
            dy, dz = (dp, dq) if half == 0 else (dq, dp)
            kk = lax.rem(z + dz + 8, 4) * 4 + lax.rem(y + dy + 8, 4)
            return self.view(half, kk, c, part)

        def nb(self, half, dp, dq):
            dy, dz = (dp, dq) if half == 0 else (dq, dp)
            return dev(sp_of(z + dz, y + dy), x)

        def go(self, half, ref, d):
            return push(ref, ref, d)

        def share(self, half, ref):
            self.sibs.append(push(ref, ref, dev(sib, x)))

        def s0(self):
            for half in (0, 1):
                h = self.h[half]
                b = self.at(half, 0, 0)
                h["p+"] = self.go(half, b, self.nb(half, 1, 0))
                h["p-"] = self.go(half, b, self.nb(half, -1, 0))
            for half in (0, 1):
                h = self.h[half]
                b = self.at(half, 0, 0)
                h["q+", 0] = self.go(half, b, self.nb(half, 0, 1))
                h["q-", 0] = self.go(half, b, self.nb(half, 0, -1))
                self.share(half, b)

        def s1(self):
            for half in (0, 1):
                h = self.h[half]
                h["p+"].wait_recv()
                h["p+f"] = self.go(half, self.at(half, -1, 0, 0), self.nb(half, 1, 0))
                h["p-"].wait_recv()
                h["p-f"] = self.go(half, self.at(half, 1, 0, 1), self.nb(half, -1, 0))
            for half in (0, 1):
                h = self.h[half]
                for dp in (-1, 1):
                    b = self.at(half, dp, 0)
                    h["q+", dp] = self.go(half, b, self.nb(half, 0, 1))
                    h["q-", dp] = self.go(half, b, self.nb(half, 0, -1))
                    self.share(half, b)

        def s2(self):
            for half in (0, 1):
                h = self.h[half]
                h["p+f"].wait_recv()
                h["p-f"].wait_recv()
                b = self.at(half, 2, 0)
                h["q+", 2] = self.go(half, b, self.nb(half, 0, 1))
                h["q-", 2] = self.go(half, b, self.nb(half, 0, -1))
                self.share(half, b)

        def s3(self, dps=(0, -1, 1, 2)):
            for dp in dps:
                for half in (0, 1):
                    h = self.h[half]
                    h["q+", dp].wait_recv()
                    b = self.at(half, dp, -1)
                    if dp in (0, 1):
                        h["f", dp] = self.go(half, b, self.nb(half, 0, 1))
                    self.share(half, b)
                    h["q-", dp].wait_recv()
                    b = self.at(half, dp, 1)
                    if dp in (2, -1):
                        h["f", dp] = self.go(half, b, self.nb(half, 0, -1))
                    self.share(half, b)

        def s4(self):
            for dp in (0, -1, 1, 2):
                for half in (0, 1):
                    self.h[half]["f", dp].wait_recv()
                    self.share(half, self.at(half, dp, 2))

        def s5(self):
            for s in self.sibs:
                s.wait_recv()

    g_o, g_u, g_d = Gather(ow_view), Gather(wu_view), Gather(wd_view)

    for cp in ow_x:
        cp.wait_recv()
    g_o.s0()
    l_wg.wait()
    l_wv.wait()
    g_u.s0()

    h_kv.wait_recv()
    h_drow.wait_recv()
    h_dcol.wait_recv()
    er = lax.broadcasted_iota(jnp.int32, (128, 2048), 0)
    ec = lax.broadcasted_iota(jnp.int32, (128, 2048), 1)
    sel = (
        ((er >> 6) == (ec >> 10))
        & ((er & 63) == (ec & 63))
        & (((ec >> 8) & 3) == ((ec >> 6) & 3))
    )
    place = jnp.where(sel, 1.0, 0.0).astype(BF16)

    def expand(i, _):
        r = pl.ds(pl.multiple_of(i * 128, 128), 128)
        kvz[r, :] = ceil_dot(kv[r, :], place).astype(BF16)
        return 0

    lax.fori_loop(0, 9, expand, 0)

    first = sp == 0
    t_ids = lax.broadcasted_iota(jnp.int32, (ROWS, 128), 0)
    center = dcol[HALO : HALO + ROWS, :]
    ok1 = (dcol[HALO - 1 : HALO - 1 + ROWS, :] == center) & ((t_ids >= 1) | jnp.logical_not(first))
    ok2 = (dcol[HALO - 2 : HALO - 2 + ROWS, :] == center) & ((t_ids >= 2) | jnp.logical_not(first))
    m1[...] = jnp.where(ok1, 1.0, 0.0)
    m2[...] = jnp.where(ok2, 1.0, 0.0)

    l_q.wait()

    ri = lax.broadcasted_iota(jnp.int32, (128, 128), 0)
    ci = lax.broadcasted_iota(jnp.int32, (128, 128), 1)

    def attend(b):
        r0 = pl.multiple_of(b * 128, 128)
        qb = q[pl.ds(r0, 128), :]
        keys = pl.ds(r0, 256)
        dq = dcol[pl.ds(pl.multiple_of(HALO + b * 128, 8), 128), :]
        k0 = drow[pl.ds(7 + b, 1), :]
        k1 = drow[pl.ds(8 + b, 1), :]
        there = jnp.logical_not(first & (b == 0))
        lower = (dq == k0) & (ci > ri) & there
        upper = (dq == k1) & (ci <= ri)
        keep = jnp.concatenate([lower, upper], axis=1)
        o = jnp.zeros((128, 256), F32)
        for h in range(4):
            s = nt_dot(qb, kvz[keys, h * 256 : (h + 1) * 256]) * (HEAD_DIM**-0.5)
            s = jnp.where(keep, s, -jnp.inf)
            sink = sinks[h]
            peak = jnp.maximum(jnp.max(s, axis=-1, keepdims=True), sink)
            e = jnp.exp(s - peak)
            total = jnp.sum(e, axis=-1, keepdims=True) + jnp.exp(sink - peak)
            p = (e / total).astype(BF16)
            o = o + ceil_dot(p, kvz[keys, 1024 + h * 256 : 1024 + (h + 1) * 256])
        att[pl.ds(r0, 128), :] = o.astype(BF16)

    a2a = {}
    af_col = pl.ds(pl.multiple_of(x * 256, 256), 256)
    for j in (2, 1, 3, 0):
        t = xat(j)

        def two(i, _, t=t):
            attend(t * 2 + i)
            return 0

        lax.fori_loop(0, 2, two, 0)
        rows = att.at[pl.ds(pl.multiple_of(t * 256, 256), 256)]
        if j:
            a2a[j] = push(rows, af.at[:, af_col], dev(sp, t))
        else:
            l_af = local(rows, af.at[:, af_col])
        if j == 1:
            g_o.s1()
        if j == 3:
            g_o.s2()
            g_u.s1()
    g_o.s3()
    g_u.s2()
    l_wd.wait()
    g_d.s0()
    g_o.s4()
    l_af.wait()
    for j in (1, 3, 2):
        a2a[j].wait_recv()
    g_o.s5()

    l_res.wait()
    l_gain.wait()
    l_cg.wait()
    l_cv.wait()

    def project(j, sq):
        col = pl.ds(pl.multiple_of(j * 256, 256), 256)
        w = ow[:, :, :, col].reshape(1024, 256)
        m = res[:, col].astype(F32) + ceil_dot(af[...], w)
        m = m.astype(BF16).astype(F32)
        mid[:, col] = m
        return sq + jnp.sum(m * m, axis=-1, keepdims=True)

    sq = lax.fori_loop(0, D // 256, project, jnp.zeros((BLK, 1), F32))
    inv = lax.rsqrt(sq * (1.0 / D) + 1e-06)
    for j in range(D // 256):
        col = slice(j * 256, (j + 1) * 256)
        nb[x, HALO:EXT, col] = (mid[:, col] * inv * gain[:, col]).astype(BF16)

    slot = xat(1)
    tail = nb.at[x, pl.ds(BLK, HALO)]
    t_sp = jnp.where(x == 3, sp_next, sp)
    tails = [
        push(tail, nb.at[slot, pl.ds(0, HALO)], dev(t_sp, xat(j))) for j in (1, 2, 3)
    ]
    i0 = len(copies)
    copies.append(None)
    tail0 = pltpu.make_async_remote_copy(
        src_ref=tail,
        dst_ref=nb.at[slot, pl.ds(0, HALO)],
        send_sem=send_sem.at[i0],
        recv_sem=recv_sem.at[i0],
        device_id=dev(sp_next, x),
        device_id_type=MESH,
    )
    tail0_local = pltpu.make_async_copy(tail, nb.at[slot, pl.ds(0, HALO)], loc_sem.at[len(loc)])
    loc.append(None)

    @pl.when(x == 3)
    def _():
        tail0.start()

    @pl.when(x != 3)
    def _():
        tail0_local.start()

    def half_of(i, h):
        return nb.at[i, pl.ds(HALO + h * 128, 128)]

    right, left = dev(sp, xat(1)), dev(sp, xat(3))
    n_r0 = push(half_of(x, 0), half_of(x, 0), right)
    n_l1 = push(half_of(x, 1), half_of(x, 1), left)
    n_r1 = push(half_of(x, 1), half_of(x, 1), right)
    n_l0 = push(half_of(x, 0), half_of(x, 0), left)

    g_u.s3()
    g_d.s1()
    n_r0.wait_recv()
    f_r = push(half_of(xat(3), 0), half_of(xat(3), 0), right)
    n_l1.wait_recv()
    f_l = push(half_of(xat(1), 1), half_of(xat(1), 1), left)
    g_u.s4()
    g_d.s2()
    g_u.s5()
    for cp in tails:
        cp.wait_recv()

    @pl.when(x == 3)
    def _():
        tail0.wait()

    @pl.when(x != 3)
    def _():
        tail0_local.wait()

    def up(d):
        def step(j, _):
            col = pl.ds(pl.multiple_of(j * 256, 256), 256)
            pre[:, col] = ceil_dot(nb[d], wu[:, col]).astype(BF16).astype(F32)
            return 0

        lax.fori_loop(0, 2 * HID // 256, step, 0)

    def conv(d):
        def step(j, _):
            gc = pl.ds(pl.multiple_of(j * 128, 128), 128)
            vc = pl.ds(pl.multiple_of(HID + j * 128, 128), 128)
            tg = cg[:, gc]
            tv = cv[:, gc]
            for r in range(0, BLK, 64):
                mr = pl.ds(pl.multiple_of(d * BLK + r, 64), 64)
                k1 = m1[mr, :] > 0.5
                k2 = m2[mr, :] > 0.5

                def taps(t, cc):
                    a = t[2:3] * pre[HALO + r : HALO + r + 64, cc]
                    a = a + jnp.where(k1, t[1:2] * pre[HALO - 1 + r : HALO - 1 + r + 64, cc], 0.0)
                    return a + jnp.where(
                        k2, t[0:1] * pre[HALO - 2 + r : HALO - 2 + r + 64, cc], 0.0
                    )

                g = taps(tg, gc)
                v = taps(tv, vc)
                hid[r : r + 64, gc] = (g / (1.0 + jnp.exp(-g)) * v).astype(BF16)
            return 0

        lax.fori_loop(0, HID // 128, step, 0)

    def down(store):
        def step(j, _):
            r = pl.ds(pl.multiple_of(j * 256, 256), 256)
            store(r, nt_dot(hid[...], wd[r, :]))
            return 0

        lax.fori_loop(0, D // 256, step, 0)

    top, bot = pl.ds(0, 128), pl.ds(128, 128)

    d = xat(1)
    n_l0.wait_recv()
    up(d)
    conv(d)
    g_d.s3()
    g_d.s4()
    g_d.s5()

    def store_r(col, a):
        prf[:, col] = a[:128]
        pr[bot, col] = a[128:].astype(BF16)

    down(store_r)
    s_r1 = push(pr.at[bot], rl.at[bot], right)

    d = xat(3)
    n_r1.wait_recv()
    up(d)
    conv(d)

    def store_l(col, a):
        pl_[top, col] = a[:128].astype(BF16)
        plf[:, col] = a[128:]

    down(store_l)
    s_l0 = push(pl_.at[top], rr.at[top], left)

    d = xat(2)
    f_r.wait_recv()
    f_l.wait_recv()
    up(d)
    conv(d)

    def store_f(col, a):
        pf[:, col] = a.astype(BF16)

    down(store_f)
    s_tr = push(pf.at[top], tl, right)
    s_tl = push(pf.at[bot], tr, left)

    up(x)
    conv(x)

    def store_own(col, a):
        own[:, col] = mid[:, col] + a

    down(store_own)

    s_tr.wait_recv()
    pr[top, :] = (prf[...] + tl[...].astype(F32)).astype(BF16)
    s_r0 = push(pr.at[top], rl.at[top], right)
    s_tl.wait_recv()
    pl_[bot, :] = (plf[...] + tr[...].astype(F32)).astype(BF16)
    s_l1 = push(pl_.at[bot], rr.at[bot], left)

    for cp in (s_r1, s_l0, s_r0, s_l1):
        cp.wait_recv()
    out[...] = (own[...] + rl[...].astype(F32) + rr[...].astype(F32)).astype(BF16)
    for cp in copies:
        if cp is not None:
            cp.wait_send()


def per_device(
    queries,
    keys,
    values,
    doc_ids,
    sinks,
    residual,
    out_weight,
    norm_gain,
    w_gate,
    w_value,
    conv_gate,
    conv_value,
    w_down,
):
    kv = jnp.concatenate([keys, values], axis=1)
    drow = doc_ids.reshape(8, 128)
    dcol = jnp.broadcast_to(doc_ids[:, None], (ROWS, 128))
    wdt = w_down.T
    any_spec = pl.BlockSpec(memory_space=pl.ANY)
    smem = pl.BlockSpec(memory_space=pltpu.SMEM)
    V = pltpu.VMEM
    i32 = jnp.int32
    return pl.pallas_call(
        kernel,
        out_shape=jax.ShapeDtypeStruct((BLK, D), BF16),
        in_specs=[any_spec] * 4 + [smem] + [any_spec] * 8,
        out_specs=pl.BlockSpec(memory_space=pltpu.VMEM),
        scratch_shapes=[
            V((ROWS, 256), BF16),
            V((ROWS + WINDOW, 128), BF16),
            V((ROWS + WINDOW, 2048), BF16),
            V((16, 128), i32),
            V((ROWS + HALO, 128), i32),
            V((ROWS, 128), F32),
            V((ROWS, 128), F32),
            V((ROWS, 256), BF16),
            V((BLK, 1024), BF16),
            V((4, 16, 16, D), BF16),
            V((BLK, D), BF16),
            V((BLK, D), F32),
            V((1, D), F32),
            V((4, EXT, D), BF16),
            V((D, 2 * HID), BF16),
            V((D, HID), BF16),
            V((EXT, 2 * HID), F32),
            V((BLK, HID), BF16),
            V((3, HID), F32),
            V((3, HID), F32),
            V((BLK, D), F32),
            V((BLK, D), BF16),
            V((128, D), F32),
            V((BLK, D), BF16),
            V((128, D), F32),
            V((BLK, D), BF16),
            V((BLK, D), BF16),
            V((BLK, D), BF16),
            V((128, D), BF16),
            V((128, D), BF16),
            pltpu.SemaphoreType.DMA((N_SEM,)),
            pltpu.SemaphoreType.DMA((N_SEM,)),
            pltpu.SemaphoreType.DMA((16,)),
        ],
        compiler_params=pltpu.CompilerParams(
            collective_id=0,
            has_side_effects=True,
            vmem_limit_bytes=67_000_000,
        ),
        cost_estimate=pl.CostEstimate(
            flops=20_000_000_000, bytes_accessed=10_000_000, transcendentals=4_000_000
        ),
    )(
        queries,
        kv,
        drow,
        dcol,
        sinks,
        residual,
        out_weight,
        norm_gain.reshape(1, D),
        w_gate,
        w_value,
        conv_gate,
        conv_value,
        wdt,
    )


def solution(mesh):
    return jax.shard_map(
        per_device,
        mesh=mesh,
        in_specs=(
            P("sp", "tp"),
            P("sp", "tp"),
            P("sp", "tp"),
            P("sp"),
            P("tp"),
            P(("sp", "tp"), None),
            P("tp", None),
            P(),
            P("sp", "tp"),
            P("sp", "tp"),
            P(None, "tp"),
            P(None, "tp"),
            P("tp", "sp"),
        ),
        out_specs=P(("sp", "tp"), None),
        check_vma=False,
    )
```

time: 257 us -> 153 us (0.60)
  Pallas kernels: 0 us -> 145 us
  waiting for transfers between devices: 134 us -> 0 us
  matrix products: 46.8 us -> 0 us
  starting transfers between devices: 20.8 us -> 0 us
  blocking collectives: 19.1 us -> 0 us
  between operations: 13.4 us -> 0.04 us
  other arithmetic: 13.2 us -> 0.87 us
  local copies, waits for them, and re-layouts: 8.96 us -> 4.58 us
    pallas_call x0 -> x1, Pallas kernels: none -> 145 us  [per_device(): pl.pallas_call(kernel, out_shape=jax.ShapeDtypeStruct((BLK, D), BF16), in...]
    all_to_all x1 -> x0, waiting for transfers between devices: 47.8 us -> none  [sent_to_all(): lax.all_to_all(jnp.broadcast_to(shard[None], (size, *shard.shape)), axis,...]
    dot_general x6 -> x0, matrix products: 46.8 us -> none  [the longest x1 22.3 us: per_device(): jnp.dot(hidden, lax.all_gather(w_down, 'sp', axis=1, tiled=True), preferr...]
    reduce_scatter x1 -> x0, waiting for transfers between devices: 45.4 us -> none  [per_device(): lax.psum_scatter(terms.astype(jnp.bfloat16), 'tp', scatter_dimension=0, t...]
    all_gather x3 -> x0, waiting for transfers between devices: 40 us -> none  [the longest x1 19.4 us: per_device(): lax.all_gather(w_down, 'sp', axis=1, tiled=True)]
    all_to_all x1 -> x0, blocking collectives: 19.1 us -> none  [per_device(): lax.all_to_all(head_out, 'tp', split_axis=0, concat_axis=1, tiled=True)]
    ppermute x5 -> x0, starting transfers between devices: 15.7 us -> none  [shifted(): return lax.ppermute(shard, axis, pairs)]
    convert_element_type x4 -> x0, other arithmetic: 9.02 us -> none  [the longest x2 6.13 us: convolve(): ext32 = ext_rows.astype(jnp.float32)]
  transfers between devices with their start and end apart: 10 -> 0, of which waited for: 5 -> 0; matrix products, arithmetic and copies ran while one was open for 17% -> 0% of each run, Pallas kernels for 0% -> 0%
where the time goes in v1:
time: 153 us; the launch traced here: 151 us
  Pallas kernels  145 us (95%)
  local copies, waits for them, and re-layouts  4.58 us (3%)
    pallas_call x1, Pallas kernels, per_device(): pl.pallas_call(kernel, out_shape=jax.ShapeDtypeStruct((BLK, D), BF16), in...  145 us
    unnamed x7, local copies, waits for them, and re-layouts  3.59 us

profile of v1, /device:TPU:1, one launch (start us, length us, event | category | flops | bytes accessed | tf_op | source)
XLA Modules:
  0.0 150.9 jit_solution(12177290137771648073)
XLA Ops:
  0.0 0.0 copy-start
  0.0 1.1 copy.14
  1.1 0.0 copy-done
  1.1 0.2 copy.15
  1.3 0.0 copy-start.1
  1.3 0.9 pad_maximum_fusion.kv_in
  2.2 0.0 copy-done.1
  2.2 1.0 broadcast_in_dim.2.dcol_in
  3.2 145.4 %shard_map.127 = bf16[256,2048]{1,0:T(8,128)(2,1)} custom-call(bf16[1024,256]{1,0:T(8,128)(2,1)} %q_in.1, bf16[1024,128]{1,0:T(8,128)(2,1)} %pad_maximum_fusion.kv_in, s32[8,128]{1,0:T(8,128)} %bitcast.3, s32[1024,128]{1,0:T(8,128)} %broadcast_in_dim.2.dcol_in, f32[4]{0:T(128)} %sinks.1, bf16[256,2048]{1,0:T(8,128)(2,1)} %res_in.1, bf16[256,2048]{1,0:T(8,128)(2,1)} %ow_in.1, ...), custom_call_target="tpu_custom_call" | custom-call | flops 20000000000 | bytes 10000000 | tf_op jit(solution)/shard_map/pallas_call | solution.py:573
  148.6 2.3 %copy.17 = bf16[256,2048]{1,0:T(8,128)(2,1)} copy(bf16[256,2048]{1,0:T(8,128)(2,1)} %shard_map.127) | data formatting | bytes 2097152
Async XLA Ops:
  0.0 1.1 copy-start
  1.3 0.9 copy-start.1

commit v2 on v1

v2 whole, which is shorter than its diff:
```python
import functools

import jax
import jax.numpy as jnp
from jax import lax
from jax.experimental import pallas as pl
from jax.experimental.pallas import tpu as pltpu
from jax.sharding import PartitionSpec as P

HEAD_DIM = 64
WINDOW = 128
MESH = pl.DeviceIdType.MESH
F32 = jnp.float32
BF16 = jnp.bfloat16
NT = (((1,), (1,)), ((), ()))

N_SP = 32
ROWS = 1024
BLK = 256
D = 2048
HID = 1408
HALO = 16
EXT = BLK + HALO
N_SEM = 256
RIGHT, LEFT, OWN, ACROSS = 0, 1, 2, 3
SLOT = {0: OWN, 1: RIGHT, 2: ACROSS, 3: LEFT}
TN = (((0,), (0,)), ((), ()))


def ceil_dot(a, b):
    return jnp.dot(a, b, preferred_element_type=F32)


def nt_dot(a, b):
    return lax.dot_general(a, b, NT, preferred_element_type=F32)


def kernel(
    q_in,
    k_in,
    v_in,
    drow_in,
    sinks,
    res_in,
    ow_in,
    gain_in,
    wg_in,
    wv_in,
    cg_in,
    cv_in,
    wd_in,
    out,
    q,
    kvt,
    kvz,
    drow,
    dcol,
    m1,
    m2,
    att,
    af,
    ow,
    res,
    mid,
    gain,
    nb,
    wu,
    wd,
    pre,
    hid,
    cg,
    cv,
    pr,
    prf,
    pl_,
    plf,
    pf,
    rl,
    rr,
    tl,
    tr,
    send_sem,
    recv_sem,
    loc_sem,
):
    sp = lax.axis_index("sp")
    x = lax.axis_index("tp")
    c = lax.rem(sp, 2)
    k = lax.div(sp, 2)
    y = lax.rem(k, 4)
    z = lax.div(k, 4)

    def sp_of(zz, yy):
        return (lax.rem(zz + 8, 4) * 4 + lax.rem(yy + 8, 4)) * 2 + c

    def xat(j):
        return lax.rem(x + j + 4, 4)

    def dev(s, t):
        return {"sp": s, "tp": t}

    sp_next = lax.rem(sp + 1, N_SP)
    sp_prev = lax.rem(sp + N_SP - 1, N_SP)
    sib = sp + 1 - 2 * c
    right, left = dev(sp, xat(1)), dev(sp, xat(3))

    scopes = []

    def phase(name):
        if scopes:
            scopes.pop().__exit__(None, None, None)
        if name:
            scopes.append(jax.named_scope(name))
            scopes[-1].__enter__()

    phase("local")
    bar = pltpu.get_barrier_semaphore()

    def hello(d):
        pl.semaphore_signal(bar, inc=1, device_id=d, device_id_type=MESH)

    for j in (1, 2, 3):
        hello(dev(sp, xat(j)))
    for dz, dy in ((0, 1), (0, -1), (1, 0), (-1, 0)):
        hello(dev(sp_of(z + dz, y + dy), x))
    hello(dev(sib, x))
    for j in range(4):
        hello(dev(sp_prev, xat(j)))

    loc = []

    def local(src, dst):
        cp = pltpu.make_async_copy(src, dst, loc_sem.at[len(loc)])
        cp.start()
        loc.append(cp)
        return cp

    l_k = local(k_in, kvt.at[pl.ds(0, 64), pl.ds(WINDOW, ROWS)])
    l_v = local(v_in, kvt.at[pl.ds(64, 64), pl.ds(WINDOW, ROWS)])
    l_drow = local(drow_in, drow.at[pl.ds(8, 8)])
    l_ow = local(ow_in, ow.at[x])
    row64 = pl.ds(pl.multiple_of(sp * 64, 64), 64)
    l_wg = local(wg_in, wu.at[row64, pl.ds(0, HID)])
    l_wv = local(wv_in, wu.at[row64, pl.ds(HID, HID)])
    l_q = local(q_in, q)
    l_wd = local(wd_in, wd.at[row64])
    l_res = local(res_in, res)
    l_gain = local(gain_in, gain)
    l_cg = local(cg_in, cg)
    l_cv = local(cv_in, cv)

    phase("barrier")
    pl.semaphore_wait(bar, 12)

    phase("send0")
    copies = []

    def push(src, dst, d):
        i = len(copies)
        cp = pltpu.make_async_remote_copy(
            src_ref=src,
            dst_ref=dst,
            send_sem=send_sem.at[i],
            recv_sem=recv_sem.at[i],
            device_id=d,
            device_id_type=MESH,
        )
        cp.start()
        copies.append(cp)
        return cp

    l_k.wait()
    l_v.wait()
    l_drow.wait()
    nxt = dev(sp_next, x)
    h_kv = push(kvt.at[:, pl.ds(ROWS, WINDOW)], kvt.at[:, pl.ds(0, WINDOW)], nxt)
    h_drow = push(drow.at[pl.ds(8, 8)], drow.at[pl.ds(0, 8)], nxt)

    def wu_view(half, kk, cc, part):
        r = (kk * 2 + cc) * 64
        n = 64 if part is None else 32
        if part == 1:
            r = r + 32
        return wu.at[pl.ds(pl.multiple_of(r, 32), n), pl.ds(half * HID, HID)]

    def wd_view(half, kk, cc, part):
        r = (kk * 2 + cc) * 64 + 32 * half
        n = 32 if part is None else 16
        if part == 1:
            r = r + 16
        return wd.at[pl.ds(pl.multiple_of(r, 16), n)]

    def go(ref, d):
        return push(ref, ref, d)

    def yz(half, n):
        dy, dz = (n, 0) if half == 0 else (0, n)
        return dev(sp_of(z + dz, y + dy), x)

    class Gather:
        def __init__(self, view):
            self.view = view
            self.sibs = []
            self.h = [{}, {}]

        def at(self, half, dp, dq, part=None):
            dy, dz = (dp, dq) if half == 0 else (dq, dp)
            kk = lax.rem(z + dz + 8, 4) * 4 + lax.rem(y + dy + 8, 4)
            return self.view(half, kk, c, part)

        def p(self, half, n):
            return yz(half, n)

        def q(self, half, n):
            return yz(1 - half, n)

        def share(self, ref):
            self.sibs.append(go(ref, dev(sib, x)))

        def s0(self):
            for half in (0, 1):
                h = self.h[half]
                b = self.at(half, 0, 0)
                h["p+"] = go(b, self.p(half, 1))
                h["p-"] = go(b, self.p(half, -1))
            self.s1q(0)

        def s1p(self):
            for half in (0, 1):
                h = self.h[half]
                h["p+"].wait_recv()
                h["p+f"] = go(self.at(half, -1, 0, 0), self.p(half, 1))
                h["p-"].wait_recv()
                h["p-f"] = go(self.at(half, 1, 0, 1), self.p(half, -1))

        def s1q(self, dp):
            for half in (0, 1):
                h = self.h[half]
                b = self.at(half, dp, 0)
                h["q+", dp] = go(b, self.q(half, 1))
                h["q-", dp] = go(b, self.q(half, -1))
                self.share(b)

        def s2(self):
            for half in (0, 1):
                h = self.h[half]
                h["p+f"].wait_recv()
                h["p-f"].wait_recv()
            self.s1q(2)

        def s3(self, dps=(0, -1, 1, 2)):
            for dp in dps:
                for half in (0, 1):
                    h = self.h[half]
                    h["q+", dp].wait_recv()
                    b = self.at(half, dp, -1)
                    if dp in (0, 1):
                        h["f", dp] = go(b, self.q(half, 1))
                    self.share(b)
                    h["q-", dp].wait_recv()
                    b = self.at(half, dp, 1)
                    if dp in (2, -1):
                        h["f", dp] = go(b, self.q(half, -1))
                    self.share(b)

        def s4(self):
            for dp in (0, -1, 1, 2):
                for half in (0, 1):
                    self.h[half]["f", dp].wait_recv()
                    self.share(self.at(half, dp, 2))

        def s5(self):
            for s in self.sibs:
                s.wait_recv()

    class GatherOut:
        def __init__(self):
            self.sibs = []
            self.h = {}

        def at(self, j, half, n=0, part=None):
            pos = lax.rem((y if half == 0 else z) + n + 8, 4)
            r = half * 128 + pos * 32
            rows = 32 if part is None else 16
            if part == 1:
                r = r + 16
            cols = pl.ds(pl.multiple_of(c * 1024, 1024), 1024)
            return ow.at[xat(j), pl.ds(pl.multiple_of(r, 16), rows), cols]

        def share(self, ref):
            self.sibs.append(go(ref, dev(sib, x)))

        def spread(self, j, half):
            b = self.at(j, half)
            self.h["+", j, half] = go(b, yz(half, 1))
            self.h["-", j, half] = go(b, yz(half, -1))
            self.share(b)

        def s0(self):
            h = self.h
            h["r", 0] = go(self.at(0, 0), right)
            h["l", 1] = go(self.at(0, 1), left)
            h["r", 1] = go(self.at(0, 1), right)
            h["l", 0] = go(self.at(0, 0), left)

        def s1(self):
            h = self.h
            h["r", 0].wait_recv()
            h["rf"] = go(self.at(3, 0), right)
            self.spread(3, 0)
            h["l", 1].wait_recv()
            h["lf"] = go(self.at(1, 1), left)
            self.spread(1, 1)
            h["r", 1].wait_recv()
            self.spread(3, 1)
            h["l", 0].wait_recv()
            self.spread(1, 0)

        def s2(self):
            self.h["rf"].wait_recv()
            self.spread(2, 0)
            self.h["lf"].wait_recv()
            self.spread(2, 1)

        def s3(self):
            h = self.h
            for j, half in ((3, 0), (1, 1), (3, 1), (1, 0), (2, 0), (2, 1)):
                h["+", j, half].wait_recv()
                h["+f", j, half] = go(self.at(j, half, -1, 0), yz(half, 1))
                self.share(self.at(j, half, -1))
                h["-", j, half].wait_recv()
                h["-f", j, half] = go(self.at(j, half, 1, 1), yz(half, -1))
                self.share(self.at(j, half, 1))

        def s4(self):
            h = self.h
            for j, half in ((3, 0), (1, 1), (3, 1), (1, 0), (2, 0), (2, 1)):
                h["+f", j, half].wait_recv()
                h["-f", j, half].wait_recv()
                self.share(self.at(j, half, 2))

        def s5(self):
            for s in self.sibs:
                s.wait_recv()

    g_o, g_u, g_d = GatherOut(), Gather(wu_view), Gather(wd_view)

    l_ow.wait()
    g_o.s0()
    l_wg.wait()
    l_wv.wait()
    g_u.s0()

    phase("expand")
    er = lax.broadcasted_iota(jnp.int32, (128, 2048), 0)
    ec = lax.broadcasted_iota(jnp.int32, (128, 2048), 1)
    sel = (
        ((er >> 6) == (ec >> 10))
        & ((er & 63) == (ec & 63))
        & (((ec >> 8) & 3) == ((ec >> 6) & 3))
    )
    place = jnp.where(sel, 1.0, 0.0).astype(BF16)

    def expand(i, _):
        r = pl.ds(pl.multiple_of(i * 128, 128), 128)
        kvz[r, :] = lax.dot_general(kvt[:, r], place, TN, preferred_element_type=F32).astype(BF16)
        return 0

    def column(i, _):
        r = pl.ds(pl.multiple_of(HALO + i * 128, 8), 128)
        dcol[r, :] = jnp.broadcast_to(drow[pl.ds(8 + i, 1), :].astype(F32), (128, 128)).T
        return 0

    lax.fori_loop(1, 9, expand, 0)
    lax.fori_loop(0, 8, column, 0)
    phase("o1")
    g_o.s1()
    phase("wait_halo")
    h_kv.wait_recv()
    h_drow.wait_recv()
    phase("masks")
    expand(0, 0)
    ahead = jnp.broadcast_to(drow[7:8, :].astype(F32), (128, 128)).T
    dcol[0:HALO, :] = ahead[128 - HALO :, :]

    first = sp == 0
    t_ids = lax.broadcasted_iota(jnp.int32, (ROWS, 128), 0)
    center = dcol[HALO : HALO + ROWS, :]
    ok1 = (dcol[HALO - 1 : HALO - 1 + ROWS, :] == center) & ((t_ids >= 1) | jnp.logical_not(first))
    ok2 = (dcol[HALO - 2 : HALO - 2 + ROWS, :] == center) & ((t_ids >= 2) | jnp.logical_not(first))
    m1[...] = jnp.where(ok1, 1.0, 0.0)
    m2[...] = jnp.where(ok2, 1.0, 0.0)

    l_q.wait()

    ri = lax.broadcasted_iota(jnp.int32, (128, 128), 0)
    ci = lax.broadcasted_iota(jnp.int32, (128, 128), 1)

    def attend(b):
        r0 = pl.multiple_of(b * 128, 128)
        qb = q[pl.ds(r0, 128), :]
        keys = pl.ds(r0, 256)
        dq = dcol[pl.ds(pl.multiple_of(HALO + b * 128, 8), 128), :]
        k0 = drow[pl.ds(7 + b, 1), :].astype(F32)
        k1 = drow[pl.ds(8 + b, 1), :].astype(F32)
        there = jnp.logical_not(first & (b == 0))
        lower = (dq == k0) & (ci > ri) & there
        upper = (dq == k1) & (ci <= ri)
        keep = jnp.concatenate([lower, upper], axis=1)
        o = jnp.zeros((128, 256), F32)
        for h in range(4):
            s = nt_dot(qb, kvz[keys, h * 256 : (h + 1) * 256]) * (HEAD_DIM**-0.5)
            s = jnp.where(keep, s, -jnp.inf)
            sink = sinks[h]
            peak = jnp.maximum(jnp.max(s, axis=-1, keepdims=True), sink)
            e = jnp.exp(s - peak)
            total = jnp.sum(e, axis=-1, keepdims=True) + jnp.exp(sink - peak)
            p = (e / total).astype(BF16)
            o = o + ceil_dot(p, kvz[keys, 1024 + h * 256 : 1024 + (h + 1) * 256])
        att[pl.ds(r0, 128), :] = o.astype(BF16)

    a2a = {}
    af_col = pl.ds(pl.multiple_of(x * 256, 256), 256)
    for j in (2, 1, 3, 0):
        t = xat(j)

        def two(i, _, t=t):
            attend(t * 2 + i)
            return 0

        phase(f"attend{j}")
        lax.fori_loop(0, 2, two, 0)
        rows = att.at[pl.ds(pl.multiple_of(t * 256, 256), 256)]
        if j:
            a2a[j] = push(rows, af.at[:, af_col], dev(sp, t))
        else:
            l_af = local(rows, af.at[:, af_col])
        if j == 2:
            phase("o2")
            g_o.s2()
        if j == 1:
            phase("u1p")
            g_u.s1p()
            g_u.s1q(-1)
        if j == 3:
            phase("o3")
            g_o.s3()
            phase("u1q")
            g_u.s1q(1)
    phase("o4")
    g_o.s4()
    phase("u2")
    g_u.s2()
    phase("a2a")
    l_af.wait()
    for j in (1, 3, 2):
        a2a[j].wait_recv()
    phase("o5")
    g_o.s5()

    phase("project")
    l_res.wait()
    l_gain.wait()
    l_cg.wait()
    l_cv.wait()

    def project(j, sq):
        col = pl.ds(pl.multiple_of(j * 512, 512), 512)
        w = ow[:, :, col].reshape(1024, 512)
        m = res[:, col].astype(F32) + ceil_dot(af[...], w)
        m = m.astype(BF16).astype(F32)
        mid[:, col] = m
        return sq + jnp.sum(m * m, axis=-1, keepdims=True)

    sq = lax.fori_loop(0, D // 512, project, jnp.zeros((BLK, 1), F32))
    inv = lax.rsqrt(sq * (1.0 / D) + 1e-06)
    for j in range(D // 256):
        col = slice(j * 256, (j + 1) * 256)
        nb[OWN, HALO:EXT, col] = (mid[:, col] * inv * gain[:, col]).astype(BF16)

    phase("send_n")
    tail = nb.at[OWN, pl.ds(BLK, HALO)]
    t_sp = jnp.where(x == 3, sp_next, sp)

    def halo_of(slot):
        return nb.at[slot, pl.ds(0, HALO)]

    tails = [push(tail, halo_of(SLOT[(1 - j) % 4]), dev(t_sp, xat(j))) for j in (1, 2, 3)]
    i0 = len(copies)
    copies.append(None)
    tail0 = pltpu.make_async_remote_copy(
        src_ref=tail,
        dst_ref=halo_of(SLOT[1]),
        send_sem=send_sem.at[i0],
        recv_sem=recv_sem.at[i0],
        device_id=dev(sp_next, x),
        device_id_type=MESH,
    )
    tail0_local = pltpu.make_async_copy(tail, halo_of(SLOT[1]), loc_sem.at[len(loc)])
    loc.append(None)

    @pl.when(x == 3)
    def _():
        tail0.start()

    @pl.when(x != 3)
    def _():
        tail0_local.start()

    def half_of(slot, h):
        return nb.at[slot, pl.ds(HALO + h * 128, 128)]

    n_r0 = push(half_of(OWN, 0), half_of(LEFT, 0), right)
    n_l1 = push(half_of(OWN, 1), half_of(RIGHT, 1), left)
    n_r1 = push(half_of(OWN, 1), half_of(LEFT, 1), right)
    n_l0 = push(half_of(OWN, 0), half_of(RIGHT, 0), left)

    phase("d0")
    l_wd.wait()
    g_d.s0()
    phase("u3")
    g_u.s3()
    phase("d1")
    g_d.s1p()
    g_d.s1q(-1)
    g_d.s1q(1)
    phase("d2")
    g_d.s2()
    phase("n_half")
    n_r0.wait_recv()
    f_r = push(half_of(LEFT, 0), half_of(ACROSS, 0), right)
    n_l1.wait_recv()
    f_l = push(half_of(RIGHT, 1), half_of(ACROSS, 1), left)
    phase("u4")
    g_u.s4()
    phase("d3")
    g_d.s3()
    phase("u5")
    g_u.s5()
    phase("tails")
    for cp in tails:
        cp.wait_recv()

    @pl.when(x == 3)
    def _():
        tail0.wait()

    @pl.when(x != 3)
    def _():
        tail0_local.wait()

    def up(slot, n):
        rows = nb[slot : slot + n].reshape(n * EXT, D)
        for h in (0, 1):
            col = pl.ds(h * HID, HID)
            pre[: n * EXT, col] = ceil_dot(rows, wu[:, col]).astype(BF16).astype(F32)

    def conv(slot, base, d):
        def step(j, _):
            gc = pl.ds(pl.multiple_of(j * 128, 128), 128)
            vc = pl.ds(pl.multiple_of(HID + j * 128, 128), 128)
            tg = cg[:, gc]
            tv = cv[:, gc]
            for r in range(0, BLK, 64):
                mr = pl.ds(pl.multiple_of(d * BLK + r, 64), 64)
                k1 = m1[mr, :] > 0.5
                k2 = m2[mr, :] > 0.5
                r0 = base * EXT + HALO + r

                def taps(t, cc):
                    a = t[2:3] * pre[r0 : r0 + 64, cc]
                    a = a + jnp.where(k1, t[1:2] * pre[r0 - 1 : r0 + 63, cc], 0.0)
                    return a + jnp.where(k2, t[0:1] * pre[r0 - 2 : r0 + 62, cc], 0.0)

                g = taps(tg, gc)
                v = taps(tv, vc)
                hid[slot, r : r + 64, gc] = (g / (1.0 + jnp.exp(-g)) * v).astype(BF16)
            return 0

        lax.fori_loop(0, HID // 128, step, 0)

    chunks = (pl.ds(0, 1024), pl.ds(1024, 1024))
    top, bot = pl.ds(0, 128), pl.ds(128, 128)

    phase("up0")
    up(OWN, 1)
    phase("conv0")
    conv(OWN, 0, x)
    phase("d4")
    g_d.s4()

    phase("wait_n1")
    n_l0.wait_recv()
    n_r1.wait_recv()
    phase("up13")
    up(RIGHT, 2)
    phase("conv13")
    conv(RIGHT, 0, xat(1))
    conv(LEFT, 1, xat(3))
    phase("d5")
    g_d.s5()
    phase("down13")
    s_one, s_two, s_three = [], [], []
    for col in chunks:
        a = nt_dot(hid[0:2].reshape(2 * BLK, HID), wd[col, :])
        prf[:, col] = a[:128]
        pr[bot, col] = a[128:256].astype(BF16)
        pl_[top, col] = a[256:384].astype(BF16)
        plf[:, col] = a[384:]
        s_one.append(push(pr.at[bot, col], rl.at[bot, col], right))
        s_one.append(push(pl_.at[top, col], rr.at[top, col], left))

    phase("wait_n2")
    f_r.wait_recv()
    f_l.wait_recv()
    phase("up2")
    up(ACROSS, 1)
    phase("conv2")
    conv(ACROSS, 0, xat(2))
    phase("down2")
    for col in chunks:
        pf[:, col] = nt_dot(hid[ACROSS], wd[col, :]).astype(BF16)
        s_two.append(
            (
                push(pf.at[top, col], tl.at[:, col], right),
                push(pf.at[bot, col], tr.at[:, col], left),
            )
        )

    phase("down0")
    for col in chunks:
        mid[:, col] += nt_dot(hid[OWN], wd[col, :])

    for i, col in enumerate(chunks):
        phase("wait_t")
        s_two[i][0].wait_recv()
        pr[top, col] = (prf[:, col] + tl[:, col].astype(F32)).astype(BF16)
        s_three.append(push(pr.at[top, col], rl.at[top, col], right))
        s_two[i][1].wait_recv()
        pl_[bot, col] = (plf[:, col] + tr[:, col].astype(F32)).astype(BF16)
        s_three.append(push(pl_.at[bot, col], rr.at[bot, col], left))

    phase("wait_s1")
    for cp in s_one:
        cp.wait_recv()
    for i, col in enumerate(chunks):
        phase("wait_s3")
        s_three[2 * i].wait_recv()
        s_three[2 * i + 1].wait_recv()
        phase("final")
        out[:, col] = (mid[:, col] + rl[:, col].astype(F32) + rr[:, col].astype(F32)).astype(BF16)
    phase("wait_sends")
    for cp in copies:
        if cp is not None:
            cp.wait_send()
    phase(None)


def per_device(
    queries,
    keys,
    values,
    doc_ids,
    sinks,
    residual,
    out_weight,
    norm_gain,
    w_gate,
    w_value,
    conv_gate,
    conv_value,
    w_down,
):
    drow = doc_ids.reshape(8, 128)
    wdt = w_down.T
    any_spec = pl.BlockSpec(memory_space=pl.ANY)
    smem = pl.BlockSpec(memory_space=pltpu.SMEM)
    V = pltpu.VMEM
    i32 = jnp.int32
    return pl.pallas_call(
        kernel,
        out_shape=jax.ShapeDtypeStruct((BLK, D), BF16),
        in_specs=[any_spec] * 4 + [smem] + [any_spec] * 8,
        out_specs=pl.BlockSpec(memory_space=pltpu.VMEM),
        scratch_shapes=[
            V((ROWS, 256), BF16),
            V((128, ROWS + WINDOW), BF16),
            V((ROWS + WINDOW, 2048), BF16),
            V((16, 128), i32),
            V((ROWS + HALO, 128), F32),
            V((ROWS, 128), F32),
            V((ROWS, 128), F32),
            V((ROWS, 256), BF16),
            V((BLK, 1024), BF16),
            V((4, 256, D), BF16),
            V((BLK, D), BF16),
            V((BLK, D), F32),
            V((1, D), F32),
            V((4, EXT, D), BF16),
            V((D, 2 * HID), BF16),
            V((D, HID), BF16),
            V((2 * EXT, 2 * HID), F32),
            V((4, BLK, HID), BF16),
            V((3, HID), F32),
            V((3, HID), F32),
            V((BLK, D), BF16),
            V((128, D), F32),
            V((BLK, D), BF16),
            V((128, D), F32),
            V((BLK, D), BF16),
            V((BLK, D), BF16),
            V((BLK, D), BF16),
            V((128, D), BF16),
            V((128, D), BF16),
            pltpu.SemaphoreType.DMA((N_SEM,)),
            pltpu.SemaphoreType.DMA((N_SEM,)),
            pltpu.SemaphoreType.DMA((16,)),
        ],
        compiler_params=pltpu.CompilerParams(
            collective_id=0,
            has_side_effects=True,
            vmem_limit_bytes=67_000_000,
        ),
        cost_estimate=pl.CostEstimate(
            flops=20_000_000_000, bytes_accessed=10_000_000, transcendentals=4_000_000
        ),
    )(
        queries,
        keys.T,
        values.T,
        drow,
        sinks,
        residual,
        out_weight,
        norm_gain.reshape(1, D),
        w_gate,
        w_value,
        conv_gate,
        conv_value,
        wdt,
    )


def solution(mesh):
    return jax.shard_map(
        per_device,
        mesh=mesh,
        in_specs=(
            P("sp", "tp"),
            P("sp", "tp"),
            P("sp", "tp"),
            P("sp"),
            P("tp"),
            P(("sp", "tp"), None),
            P("tp", None),
            P(),
            P("sp", "tp"),
            P("sp", "tp"),
            P(None, "tp"),
            P(None, "tp"),
            P("tp", "sp"),
        ),
        out_specs=P(("sp", "tp"), None),
        check_vma=False,
    )
```

time: 153 us -> 119 us (0.78); the launches traced: 151 us -> 119 us
  Pallas kernels: 145 us -> 116 us
  local copies, waits for them, and re-layouts: 4.58 us -> 2.3 us
    pallas_call x1, Pallas kernels: 145 us -> 116 us  [per_device(): pl.pallas_call(kernel, out_shape=jax.ShapeDtypeStruct((BLK, D), BF16), in...]
    unnamed x7 -> x1, local copies, waits for them, and re-layouts: 3.59 us -> 2.3 us
where the time goes in v2:
time: 119 us
  Pallas kernels  116 us (97%)
  local copies, waits for them, and re-layouts  2.3 us (2%)
    pallas_call x1, Pallas kernels, per_device(): pl.pallas_call(kernel, out_shape=jax.ShapeDtypeStruct((BLK, D), BF16), in...  116 us

profile of v2, /device:TPU:1, one launch (start us, length us, event | category | flops | bytes accessed | tf_op | source)
XLA Modules:
  0.0 118.7 jit_solution(13940133545828834688)
XLA Ops:
  0.0 116.4 %shard_map.127 = bf16[256,2048]{1,0:T(8,128)(2,1)} custom-call(bf16[1024,256]{1,0:T(8,128)(2,1)} %q_in.1, bf16[64,1024]{1,0:T(8,128)(2,1)} %bitcast.6, bf16[64,1024]{1,0:T(8,128)(2,1)} %bitcast.7, s32[8,128]{1,0:T(8,128)} %bitcast.9, f32[4]{0:T(128)} %sinks.1, bf16[256,2048]{1,0:T(8,128)(2,1)} %res_in.1, bf16[256,2048]{1,0:T(8,128)(2,1)} %ow_in.1, ...), custom_call_target="tpu_custom_call" | custom-call | flops 20000000000 | bytes 10000000 | tf_op jit(solution)/shard_map/pallas_call | solution.py:680
  116.4 2.3 %copy.15 = bf16[256,2048]{1,0:T(8,128)(2,1)} copy(bf16[256,2048]{1,0:T(8,128)(2,1)} %shard_map.127) | data formatting | bytes 2097152

commit v3 on v2

v3 whole, which is shorter than its diff:
```python
import functools

import jax
import jax.numpy as jnp
from jax import lax
from jax.experimental import pallas as pl
from jax.experimental.pallas import tpu as pltpu
from jax.sharding import PartitionSpec as P

HEAD_DIM = 64
WINDOW = 128
MESH = pl.DeviceIdType.MESH
F32 = jnp.float32
BF16 = jnp.bfloat16
NT = (((1,), (1,)), ((), ()))

N_SP = 32
ROWS = 1024
BLK = 256
D = 2048
HID = 1408
HALO = 8
HALF = BLK // 2
EXT = HALF + HALO
PAIR = 2 * EXT
N_SEND, N_RECV = 40, 64
R1, L0, R0, L1, O0, O1, A0, A1 = range(8)
FIRST = {0: O0, 1: R0, 2: A0, 3: L0}
TN = (((0,), (0,)), ((), ()))


def ceil_dot(a, b):
    return jnp.dot(a, b, preferred_element_type=F32)


def nt_dot(a, b):
    return lax.dot_general(a, b, NT, preferred_element_type=F32)


def kernel(
    q_in,
    k_in,
    v_in,
    drow_in,
    sinks,
    res_in,
    ow_in,
    gain_in,
    wg_in,
    wv_in,
    cg_in,
    cv_in,
    wd_in,
    out,
    q,
    kvt,
    kvz,
    drow,
    dcol,
    m1,
    m2,
    att,
    af,
    ow,
    res,
    mid,
    gain,
    nb,
    wu,
    wd,
    pre,
    hid,
    cg,
    cv,
    s1,
    s2,
    s3,
    p3,
    rl,
    rr,
    tl,
    tr,
    send_sem,
    recv_sem,
    loc_sem,
):
    sp = lax.axis_index("sp")
    x = lax.axis_index("tp")
    c = lax.rem(sp, 2)
    k = lax.div(sp, 2)
    y = lax.rem(k, 4)
    z = lax.div(k, 4)

    def sp_of(zz, yy):
        return (lax.rem(zz + 8, 4) * 4 + lax.rem(yy + 8, 4)) * 2 + c

    def xat(j):
        return lax.rem(x + j + 4, 4)

    def dev(s, t):
        return {"sp": s, "tp": t}

    sp_next = lax.rem(sp + 1, N_SP)
    sp_prev = lax.rem(sp + N_SP - 1, N_SP)
    sib = sp + 1 - 2 * c
    right, left = dev(sp, xat(1)), dev(sp, xat(3))

    scopes = []

    def phase(name):
        if scopes:
            scopes.pop().__exit__(None, None, None)
        if name:
            scopes.append(jax.named_scope(name))
            scopes[-1].__enter__()

    phase("local")
    bar = pltpu.get_barrier_semaphore()

    def hello(d):
        pl.semaphore_signal(bar, inc=1, device_id=d, device_id_type=MESH)

    for j in (1, 2, 3):
        hello(dev(sp, xat(j)))
    for dz, dy in ((0, 1), (0, -1), (1, 0), (-1, 0)):
        hello(dev(sp_of(z + dz, y + dy), x))
    hello(dev(sib, x))
    for j in range(4):
        hello(dev(sp_prev, xat(j)))

    loc = []

    def local(src, dst):
        cp = pltpu.make_async_copy(src, dst, loc_sem.at[len(loc)])
        cp.start()
        loc.append(cp)
        return cp

    l_k = local(k_in, kvt.at[pl.ds(0, 64), pl.ds(WINDOW, ROWS)])
    l_v = local(v_in, kvt.at[pl.ds(64, 64), pl.ds(WINDOW, ROWS)])
    l_drow = local(drow_in, drow.at[pl.ds(8, 8)])
    l_ow = local(ow_in, ow.at[x])
    row64 = pl.ds(pl.multiple_of(sp * 64, 64), 64)
    l_wg = local(wg_in, wu.at[row64, pl.ds(0, HID)])
    l_wv = local(wv_in, wu.at[row64, pl.ds(HID, HID)])
    l_q = local(q_in, q)
    l_wd = local(wd_in, wd.at[row64])
    l_res = local(res_in, res)
    l_gain = local(gain_in, gain)
    l_cg = local(cg_in, cg)
    l_cv = local(cv_in, cv)

    er = lax.broadcasted_iota(jnp.int32, (128, 2048), 0)
    ec = lax.broadcasted_iota(jnp.int32, (128, 2048), 1)
    sel = (
        ((er >> 6) == (ec >> 10))
        & ((er & 63) == (ec & 63))
        & (((ec >> 8) & 3) == ((ec >> 6) & 3))
    )
    place = jnp.where(sel, 1.0, 0.0).astype(BF16)

    def column(i, _):
        r = pl.ds(pl.multiple_of(HALO + i * 128, 8), 128)
        dcol[r, :] = jnp.broadcast_to(drow[pl.ds(8 + i, 1), :].astype(F32), (128, 128)).T
        return 0

    l_drow.wait()
    lax.fori_loop(0, 8, column, 0)

    phase("barrier")
    pl.semaphore_wait(bar, 12)

    phase("send0")
    copies = []
    used = {"s": 0, "r": 0}

    def new(kind):
        used[kind] += 1
        return (send_sem if kind == "s" else recv_sem).at[used[kind] - 1]

    def push(src, dst, d, ss=None, rs=None):
        cp = pltpu.make_async_remote_copy(
            src_ref=src,
            dst_ref=dst,
            send_sem=new("s") if ss is None else ss,
            recv_sem=new("r") if rs is None else rs,
            device_id=d,
            device_id_type=MESH,
        )
        cp.start()
        if ss is None:
            copies.append(cp)
        return cp

    def wait_all(sem, view):
        pltpu.make_async_copy(view, view, sem).wait()

    l_k.wait()
    l_v.wait()
    nxt = dev(sp_next, x)
    h_kv = push(kvt.at[:, pl.ds(ROWS, WINDOW)], kvt.at[:, pl.ds(0, WINDOW)], nxt)
    h_drow = push(drow.at[pl.ds(8, 8)], drow.at[pl.ds(0, 8)], nxt)

    def wu_view(half, kk, cc, part):
        r = (kk * 2 + cc) * 64
        n = 64 if part is None else 32
        if part == 1:
            r = r + 32
        return wu.at[pl.ds(pl.multiple_of(r, 32), n), pl.ds(half * HID, HID)]

    def wd_view(half, kk, cc, part):
        r = (kk * 2 + cc) * 64 + 32 * half
        n = 32 if part is None else 16
        if part == 1:
            r = r + 16
        return wd.at[pl.ds(pl.multiple_of(r, 16), n)]

    def yz(half, n):
        dy, dz = (n, 0) if half == 0 else (0, n)
        return dev(sp_of(z + dz, y + dy), x)

    class Group:
        def __init__(self, size):
            self.size = size
            self.ss = new("s")
            self.sent = 0
            self.sem = {}
            self.due = {}

        def go(self, key, ref, units, d):
            if key not in self.sem:
                self.sem[key] = new("r")
                self.due[key] = 0
            push(ref, ref, d, self.ss, self.sem[key])
            self.due[key] += units
            self.sent += units

        def come(self, key):
            wait_all(self.sem[key], self.size(self.due[key]))

        def share(self, ref, units=2):
            self.go("sib", ref, units, dev(sib, x))

        def s5(self):
            self.come("sib")

        def gone(self):
            wait_all(self.ss, self.size(self.sent))

    class Gather(Group):
        def __init__(self, view, size):
            super().__init__(size)
            self.view = view

        def at(self, half, dp, dq, part=None):
            dy, dz = (dp, dq) if half == 0 else (dq, dp)
            kk = lax.rem(z + dz + 8, 4) * 4 + lax.rem(y + dy + 8, 4)
            return self.view(half, kk, c, part)

        def p(self, half, n):
            return yz(half, n)

        def q(self, half, n):
            return yz(1 - half, n)

        def s0p(self):
            for half in (0, 1):
                b = self.at(half, 0, 0)
                self.go("p", b, 2, self.p(half, 1))
                self.go("p", b, 2, self.p(half, -1))

        def s1p(self):
            self.come("p")
            for half in (0, 1):
                self.go("pf", self.at(half, -1, 0, 0), 1, self.p(half, 1))
                self.go("pf", self.at(half, 1, 0, 1), 1, self.p(half, -1))

        def s1q(self, dp):
            for half in (0, 1):
                b = self.at(half, dp, 0)
                self.go(("q", dp), b, 2, self.q(half, 1))
                self.go(("q", dp), b, 2, self.q(half, -1))
                self.share(b)

        def s2(self):
            self.come("pf")
            self.s1q(2)

        def s3(self, dps):
            for dp in dps:
                self.come(("q", dp))
                for half in (0, 1):
                    lo, hi = self.at(half, dp, -1), self.at(half, dp, 1)
                    if dp in (0, 1):
                        self.go("f", lo, 2, self.q(half, 1))
                    else:
                        self.go("f", hi, 2, self.q(half, -1))
                    self.share(lo)
                    self.share(hi)

        def s4(self):
            self.come("f")
            for dp in (0, -1, 1, 2):
                for half in (0, 1):
                    self.share(self.at(half, dp, 2))

    class GatherOut(Group):
        def at(self, j, par, r, n):
            r = lax.rem(y + z + par, 2) * 128 + r
            cols = pl.ds(pl.multiple_of(c * 1024, 1024), 1024)
            return ow.at[xat(j), pl.ds(pl.multiple_of(r, 32), n), cols]

        def piece(self, j, half):
            return self.at(j, 0, half * 64, 64)

        def spread(self, j, half, n):
            for i in (0, 1):
                self.go(("y", n), self.at(j, 0, half * 64 + i * 32, 32), 2, yz(half, 1 - 2 * i))
            self.share(self.piece(j, half), 4)

        def s0(self):
            self.go("x0", self.piece(0, 0), 4, right)
            self.go("x0", self.piece(0, 1), 4, left)
            self.go("x1", self.piece(0, 1), 4, right)
            self.go("x1", self.piece(0, 0), 4, left)

        def s1a(self):
            self.come("x0")
            self.go("xf", self.piece(3, 0), 4, right)
            self.go("xf", self.piece(1, 1), 4, left)
            self.spread(3, 0, 0)
            self.spread(1, 1, 0)

        def s1b(self):
            self.come("x1")
            self.spread(3, 1, 1)
            self.spread(1, 0, 1)

        def s2(self):
            self.come("xf")
            self.spread(2, 0, 2)
            self.spread(2, 1, 2)

        def s4(self, n):
            self.come(("y", n))
            for j, half in (((3, 0), (1, 1)), ((3, 1), (1, 0)), ((2, 0), (2, 1)))[n]:
                self.share(self.at(j, 1, half * 64, 64), 4)

    def ow_size(n):
        for quarters in (1, 2, 3, 4):
            if n * 8 % quarters == 0 and n * 8 // quarters <= 256:
                return ow.at[pl.ds(0, quarters), pl.ds(0, n * 8 // quarters)]

    g_o = GatherOut(ow_size)
    g_u = Gather(wu_view, lambda n: wu.at[pl.ds(0, 16 * n)])
    g_d = Gather(wd_view, lambda n: wd.at[pl.ds(0, 16 * n)])

    l_ow.wait()
    g_o.s0()
    l_wg.wait()
    l_wv.wait()
    g_u.s0p()

    phase("expand")

    def expand(i, _):
        r = pl.ds(pl.multiple_of(i * 128, 128), 128)
        kvz[r, :] = lax.dot_general(kvt[:, r], place, TN, preferred_element_type=F32).astype(BF16)
        return 0

    lax.fori_loop(1, 9, expand, 0)
    phase("o1")
    g_o.s1a()
    phase("wait_halo")
    h_kv.wait_recv()
    h_drow.wait_recv()
    phase("masks")
    expand(0, 0)
    ahead = jnp.broadcast_to(drow[7:8, :].astype(F32), (128, 128)).T
    dcol[0:HALO, :] = ahead[128 - HALO :, :]

    first = sp == 0
    t_ids = lax.broadcasted_iota(jnp.int32, (ROWS, 128), 0)
    center = dcol[HALO : HALO + ROWS, :]
    ok1 = (dcol[HALO - 1 : HALO - 1 + ROWS, :] == center) & ((t_ids >= 1) | jnp.logical_not(first))
    ok2 = (dcol[HALO - 2 : HALO - 2 + ROWS, :] == center) & ((t_ids >= 2) | jnp.logical_not(first))
    m1[...] = jnp.where(ok1, 1.0, 0.0)
    m2[...] = jnp.where(ok2, 1.0, 0.0)

    l_q.wait()

    ri = lax.broadcasted_iota(jnp.int32, (128, 128), 0)
    ci = lax.broadcasted_iota(jnp.int32, (128, 128), 1)

    def attend(b):
        r0 = pl.multiple_of(b * 128, 128)
        qb = q[pl.ds(r0, 128), :]
        keys = pl.ds(r0, 256)
        dq = dcol[pl.ds(pl.multiple_of(HALO + b * 128, 8), 128), :]
        k0 = drow[pl.ds(7 + b, 1), :].astype(F32)
        k1 = drow[pl.ds(8 + b, 1), :].astype(F32)
        there = jnp.logical_not(first & (b == 0))
        lower = (dq == k0) & (ci > ri) & there
        upper = (dq == k1) & (ci <= ri)
        keep = jnp.concatenate([lower, upper], axis=1)
        o = jnp.zeros((128, 256), F32)
        for h in range(4):
            s = nt_dot(qb, kvz[keys, h * 256 : (h + 1) * 256]) * (HEAD_DIM**-0.5)
            s = jnp.where(keep, s, -jnp.inf)
            sink = sinks[h]
            peak = jnp.maximum(jnp.max(s, axis=-1, keepdims=True), sink)
            e = jnp.exp(s - peak)
            total = jnp.sum(e, axis=-1, keepdims=True) + jnp.exp(sink - peak)
            p = (e / total).astype(BF16)
            o = o + ceil_dot(p, kvz[keys, 1024 + h * 256 : 1024 + (h + 1) * 256])
        att[pl.ds(r0, 128), :] = o.astype(BF16)

    a2a = {}
    af_col = pl.ds(pl.multiple_of(x * 256, 256), 256)
    for j in (2, 1, 3, 0):
        t = xat(j)

        def two(i, _, t=t):
            attend(t * 2 + i)
            return 0

        phase(f"attend{j}")
        lax.fori_loop(0, 2, two, 0)
        rows = att.at[pl.ds(pl.multiple_of(t * 256, 256), 256)]
        if j:
            a2a[j] = push(rows, af.at[:, af_col], dev(sp, t))
        else:
            l_af = local(rows, af.at[:, af_col])
        if j == 2:
            phase("d0p")
            l_wd.wait()
            g_d.s0p()
        if j == 1:
            phase("o1b")
            g_o.s1b()
            g_u.s1p()
        if j == 3:
            phase("o2")
            g_o.s2()
            g_u.s1q(0)
    phase("u1")
    g_u.s1q(-1)
    g_u.s1q(1)
    g_o.s4(0)
    phase("a2a")
    l_af.wait()
    for j in (1, 3, 2):
        a2a[j].wait_recv()
    phase("o4")
    g_o.s4(1)
    g_o.s4(2)
    phase("u2")
    g_u.s2()
    phase("o5")
    g_o.s5()

    phase("project")
    l_res.wait()
    l_gain.wait()
    l_cg.wait()
    l_cv.wait()

    def project(j, sq):
        col = pl.ds(pl.multiple_of(j * 512, 512), 512)
        w = ow[:, :, col].reshape(1024, 512)
        m = res[:, col].astype(F32) + ceil_dot(af[...], w)
        m = m.astype(BF16).astype(F32)
        mid[:, col] = m
        return sq + jnp.sum(m * m, axis=-1, keepdims=True)

    sq = lax.fori_loop(0, D // 512, project, jnp.zeros((BLK, 1), F32))
    inv = lax.rsqrt(sq * (1.0 / D) + 1e-06)
    for h in (0, 1):
        r = slice(h * HALF, (h + 1) * HALF)
        for j in range(D // 512):
            col = slice(j * 512, (j + 1) * 512)
            n = (mid[r, col] * inv[r] * gain[:, col]).astype(BF16)
            nb[O0 + h, HALO:EXT, col] = n
            if h == 0:
                nb[O1, 0:HALO, col] = n[HALF - HALO :]

    phase("send_n")

    def rows_of(i):
        return nb.at[i, pl.ds(HALO, HALF)]

    def halo_of(i):
        return nb.at[i, pl.ds(0, HALO)]

    tail = nb.at[O1, pl.ds(HALF, HALO)]
    t_sp = jnp.where(x == 3, sp_next, sp)
    n_mid = push(halo_of(O1), halo_of(R1), left)
    tails = [push(tail, halo_of(FIRST[(1 - j) % 4]), dev(t_sp, xat(j))) for j in (1, 3)]
    n_r0 = push(rows_of(O0), rows_of(L0), right)
    n_l1 = push(rows_of(O1), rows_of(R1), left)
    tails.append(push(tail, halo_of(FIRST[3]), dev(t_sp, xat(2))))
    tail0 = pltpu.make_async_remote_copy(
        src_ref=tail,
        dst_ref=halo_of(R0),
        send_sem=new("s"),
        recv_sem=new("r"),
        device_id=dev(sp_next, x),
        device_id_type=MESH,
    )
    tail0_local = pltpu.make_async_copy(tail, halo_of(R0), loc_sem.at[len(loc)])
    loc.append(None)

    @pl.when(x == 3)
    def _():
        tail0.start()

    @pl.when(x != 3)
    def _():
        tail0_local.start()

    n_r1 = push(rows_of(O1), rows_of(L1), right)
    n_l0 = push(rows_of(O0), rows_of(R0), left)

    phase("u3a")
    g_u.s3((0,))
    g_d.s1p()
    phase("u3b")
    g_u.s3((-1,))
    g_d.s1q(0)
    g_d.s1q(-1)
    phase("u3c")
    g_u.s3((1,))
    g_d.s1q(1)
    phase("u3d")
    g_u.s3((2,))
    phase("n_half")
    n_r0.wait_recv()
    f_r = push(rows_of(L0), rows_of(A0), right)
    n_l1.wait_recv()
    f_l = push(rows_of(R1), rows_of(A1), left)
    phase("d2")
    g_d.s2()
    phase("d3a")
    g_d.s3((0,))
    phase("u4")
    g_u.s4()
    phase("d3b")
    g_d.s3((-1, 1))
    phase("d3c")
    g_d.s3((2,))
    phase("u5")
    g_u.s5()
    phase("tails")
    n_mid.wait_recv()
    for cp in tails:
        cp.wait_recv()

    @pl.when(x == 3)
    def _():
        tail0.wait()

    @pl.when(x != 3)
    def _():
        tail0_local.wait()

    def up(i):
        rows = nb[i : i + 2].reshape(PAIR, D)
        for h in (0, 1):
            col = pl.ds(h * HID, HID)
            pre[:, col] = ceil_dot(rows, wu[:, col]).astype(BF16).astype(F32)

    def conv(i, blocks):
        def step(j, _):
            gc = pl.ds(pl.multiple_of(j * 128, 128), 128)
            vc = pl.ds(pl.multiple_of(HID + j * 128, 128), 128)
            tg = cg[:, gc]
            tv = cv[:, gc]
            for n, (d, h) in enumerate(blocks):
                for r in range(0, HALF, 64):
                    mr = pl.ds(pl.multiple_of(d * BLK + h * HALF + r, 64), 64)
                    k1 = m1[mr, :] > 0.5
                    k2 = m2[mr, :] > 0.5
                    r0 = n * EXT + HALO + r

                    def taps(t, cc):
                        a = t[2:3] * pre[r0 : r0 + 64, cc]
                        a = a + jnp.where(k1, t[1:2] * pre[r0 - 1 : r0 + 63, cc], 0.0)
                        return a + jnp.where(k2, t[0:1] * pre[r0 - 2 : r0 + 62, cc], 0.0)

                    g = taps(tg, gc)
                    v = taps(tv, vc)
                    o = n * HALF + r
                    hid[i // 2, o : o + 64, gc] = (g / (1.0 + jnp.exp(-g)) * v).astype(BF16)
            return 0

        lax.fori_loop(0, HID // 128, step, 0)

    chunks = (pl.ds(0, 1024), pl.ds(1024, 1024))
    top, bot = pl.ds(0, HALF), pl.ds(HALF, HALF)

    def down(i, col):
        return nt_dot(hid[i // 2], wd[col, :])

    phase("up0")
    up(O0)
    phase("conv0")
    conv(O0, ((x, 0), (x, 1)))

    phase("up1")
    up(R1)
    phase("d4")
    g_d.s4()
    phase("conv1")
    conv(R1, ((xat(1), 1), (xat(3), 0)))
    phase("d5")
    g_d.s5()
    phase("down1")
    s_one, s_two, s_three = [], [], []
    for col in chunks:
        a = down(R1, col)
        s1[:, col] = a.astype(BF16)
        s_one.append(push(s1.at[top, col], rl.at[bot, col], right))
        s_one.append(push(s1.at[bot, col], rr.at[top, col], left))

    phase("wait_n2")
    f_r.wait_recv()
    f_l.wait_recv()
    nb[A1, 0:HALO, :] = nb[A0, HALF:EXT, :]
    phase("up2")
    up(A0)
    phase("conv2")
    conv(A0, ((xat(2), 0), (xat(2), 1)))
    phase("down2")
    for col in chunks:
        s2[:, col] = down(A0, col).astype(BF16)
        s_two.append(
            (
                push(s2.at[top, col], tl.at[:, col], right),
                push(s2.at[bot, col], tr.at[:, col], left),
            )
        )

    phase("wait_n1")
    n_l0.wait_recv()
    n_r1.wait_recv()
    nb[L1, 0:HALO, :] = nb[L0, HALF:EXT, :]
    phase("up3")
    up(R0)
    phase("conv3")
    conv(R0, ((xat(1), 0), (xat(3), 1)))
    phase("down3")
    for col in chunks:
        p3[:, col] = down(R0, col)

    def finish(i, col):
        s_two[i][0].wait_recv()
        s3[top, col] = (p3[top, col] + tl[:, col].astype(F32)).astype(BF16)
        s_three.append(push(s3.at[top, col], rl.at[top, col], right))
        s_two[i][1].wait_recv()
        s3[bot, col] = (p3[bot, col] + tr[:, col].astype(F32)).astype(BF16)
        s_three.append(push(s3.at[bot, col], rr.at[bot, col], left))

    phase("down0")
    for col in chunks:
        mid[:, col] += down(O0, col)
    for i, col in enumerate(chunks):
        phase("wait_t")
        finish(i, col)

    phase("wait_s1")
    for cp in s_one:
        cp.wait_recv()
    for i, col in enumerate(chunks):
        phase("wait_s3")
        s_three[2 * i].wait_recv()
        s_three[2 * i + 1].wait_recv()
        phase("final")
        out[:, col] = (mid[:, col] + rl[:, col].astype(F32) + rr[:, col].astype(F32)).astype(BF16)
    phase("wait_sends")
    for cp in copies:
        cp.wait_send()
    for g in (g_o, g_u, g_d):
        g.gone()
    phase(None)
    assert used["s"] <= N_SEND and used["r"] <= N_RECV, used


def per_device(
    queries,
    keys,
    values,
    doc_ids,
    sinks,
    residual,
    out_weight,
    norm_gain,
    w_gate,
    w_value,
    conv_gate,
    conv_value,
    w_down,
):
    drow = doc_ids.reshape(8, 128)
    wdt = w_down.T
    any_spec = pl.BlockSpec(memory_space=pl.ANY)
    smem = pl.BlockSpec(memory_space=pltpu.SMEM)
    V = pltpu.VMEM
    i32 = jnp.int32
    return pl.pallas_call(
        kernel,
        out_shape=jax.ShapeDtypeStruct((BLK, D), BF16),
        in_specs=[any_spec] * 4 + [smem] + [any_spec] * 8,
        out_specs=pl.BlockSpec(memory_space=pltpu.VMEM),
        scratch_shapes=[
            V((ROWS, 256), BF16),
            V((128, ROWS + WINDOW), BF16),
            V((ROWS + WINDOW, 2048), BF16),
            V((16, 128), i32),
            V((ROWS + HALO, 128), F32),
            V((ROWS, 128), F32),
            V((ROWS, 128), F32),
            V((ROWS, 256), BF16),
            V((BLK, 1024), BF16),
            V((4, 256, D), BF16),
            V((BLK, D), BF16),
            V((BLK, D), F32),
            V((1, D), F32),
            V((8, EXT, D), BF16),
            V((D, 2 * HID), BF16),
            V((D, HID), BF16),
            V((PAIR, 2 * HID), F32),
            V((4, BLK, HID), BF16),
            V((3, HID), F32),
            V((3, HID), F32),
            V((BLK, D), BF16),
            V((BLK, D), BF16),
            V((BLK, D), BF16),
            V((BLK, D), F32),
            V((BLK, D), BF16),
            V((BLK, D), BF16),
            V((128, D), BF16),
            V((128, D), BF16),
            pltpu.SemaphoreType.DMA((N_SEND,)),
            pltpu.SemaphoreType.DMA((N_RECV,)),
            pltpu.SemaphoreType.DMA((16,)),
        ],
        compiler_params=pltpu.CompilerParams(
            collective_id=0,
            has_side_effects=True,
            vmem_limit_bytes=67_000_000,
        ),
        cost_estimate=pl.CostEstimate(
            flops=20_000_000_000, bytes_accessed=10_000_000, transcendentals=4_000_000
        ),
    )(
        queries,
        keys.T,
        values.T,
        drow,
        sinks,
        residual,
        out_weight,
        norm_gain.reshape(1, D),
        w_gate,
        w_value,
        conv_gate,
        conv_value,
        wdt,
    )


def solution(mesh):
    return jax.shard_map(
        per_device,
        mesh=mesh,
        in_specs=(
            P("sp", "tp"),
            P("sp", "tp"),
            P("sp", "tp"),
            P("sp"),
            P("tp"),
            P(("sp", "tp"), None),
            P("tp", None),
            P(),
            P("sp", "tp"),
            P("sp", "tp"),
            P(None, "tp"),
            P(None, "tp"),
            P("tp", "sp"),
        ),
        out_specs=P(("sp", "tp"), None),
        check_vma=False,
    )
```

time: 119 us -> 111 us (0.933)
  Pallas kernels: 116 us -> 108 us
    pallas_call x1, Pallas kernels: 116 us -> 108 us  [per_device(): pl.pallas_call(kernel, out_shape=jax.ShapeDtypeStruct((BLK, D), BF16), in...]
where the time goes in v3:
time: 111 us; the launch traced here: 110 us
  Pallas kernels  108 us (97%)
  local copies, waits for them, and re-layouts  2.3 us (2%)
    pallas_call x1, Pallas kernels, per_device(): pl.pallas_call(kernel, out_shape=jax.ShapeDtypeStruct((BLK, D), BF16), in...  108 us
    unnamed x1, local copies, waits for them, and re-layouts  2.3 us

profile of v3, /device:TPU:1, one launch (start us, length us, event | category | flops | bytes accessed | tf_op | source)
XLA Modules:
  0.0 110.5 jit_solution(9568061382277769578)
XLA Ops:
  0.0 108.2 %shard_map.127 = bf16[256,2048]{1,0:T(8,128)(2,1)} custom-call(bf16[1024,256]{1,0:T(8,128)(2,1)} %q_in.1, bf16[64,1024]{1,0:T(8,128)(2,1)} %bitcast.6, bf16[64,1024]{1,0:T(8,128)(2,1)} %bitcast.7, s32[8,128]{1,0:T(8,128)} %bitcast.9, f32[4]{0:T(128)} %sinks.1, bf16[256,2048]{1,0:T(8,128)(2,1)} %res_in.1, bf16[256,2048]{1,0:T(8,128)(2,1)} %ow_in.1, ...), custom_call_target="tpu_custom_call" | custom-call | flops 20000000000 | bytes 10000000 | tf_op jit(solution)/shard_map/pallas_call | solution.py:709
  108.2 2.3 %copy.15 = bf16[256,2048]{1,0:T(8,128)(2,1)} copy(bf16[256,2048]{1,0:T(8,128)(2,1)} %shard_map.127) | data formatting | bytes 2097152

commit v4 on v3

--- a/solution.py
+++ b/solution.py
@@ -26,6 +26,7 @@
 N_SEND, N_RECV = 40, 64
 R1, L0, R0, L1, O0, O1, A0, A1 = range(8)
 FIRST = {0: O0, 1: R0, 2: A0, 3: L0}
+POS = {0: 0, 1: 1, 3: 2, 2: 3}
 TN = (((0,), (0,)), ((), ()))
 
 
@@ -61,6 +62,7 @@
     m2,
     att,
     af,
+    via,
     ow,
     res,
     mid,
@@ -69,6 +71,7 @@
     wu,
     wd,
     pre,
+    pre0,
     hid,
     cg,
     cv,
@@ -139,7 +142,7 @@
     l_k = local(k_in, kvt.at[pl.ds(0, 64), pl.ds(WINDOW, ROWS)])
     l_v = local(v_in, kvt.at[pl.ds(64, 64), pl.ds(WINDOW, ROWS)])
     l_drow = local(drow_in, drow.at[pl.ds(8, 8)])
-    l_ow = local(ow_in, ow.at[x])
+    l_ow = local(ow_in, ow.at[0])
     row64 = pl.ds(pl.multiple_of(sp * 64, 64), 64)
     l_wg = local(wg_in, wu.at[row64, pl.ds(0, HID)])
     l_wv = local(wv_in, wu.at[row64, pl.ds(HID, HID)])
@@ -198,8 +201,31 @@
     l_k.wait()
     l_v.wait()
     nxt = dev(sp_next, x)
-    h_kv = push(kvt.at[:, pl.ds(ROWS, WINDOW)], kvt.at[:, pl.ds(0, WINDOW)], nxt)
-    h_drow = push(drow.at[pl.ds(8, 8)], drow.at[pl.ds(0, 8)], nxt)
+    first = sp == 0
+    last = sp == N_SP - 1
+
+    def remote(src, dst, d):
+        return pltpu.make_async_remote_copy(
+            src_ref=src,
+            dst_ref=dst,
+            send_sem=new("s"),
+            recv_sem=new("r"),
+            device_id=d,
+            device_id_type=MESH,
+        )
+
+    h_kv = remote(kvt.at[:, pl.ds(ROWS, WINDOW)], kvt.at[:, pl.ds(0, WINDOW)], nxt)
+    h_drow = remote(drow.at[pl.ds(8, 8)], drow.at[pl.ds(0, 8)], nxt)
+
+    @pl.when(jnp.logical_not(last))
+    def _():
+        h_kv.start()
+        h_drow.start()
+
+    @pl.when(first)
+    def _():
+        kvt[:, 0:WINDOW] = jnp.zeros((128, WINDOW), BF16)
+        drow[0:8, :] = jnp.zeros((8, 128), jnp.int32)
 
     def wu_view(half, kk, cc, part):
         r = (kk * 2 + cc) * 64
@@ -227,19 +253,19 @@
             self.sem = {}
             self.due = {}
 
-        def go(self, key, ref, units, d):
+        def go(self, key, ref, units, d, dst=None):
             if key not in self.sem:
                 self.sem[key] = new("r")
                 self.due[key] = 0
-            push(ref, ref, d, self.ss, self.sem[key])
+            push(ref, ref if dst is None else dst, d, self.ss, self.sem[key])
             self.due[key] += units
             self.sent += units
 
         def come(self, key):
             wait_all(self.sem[key], self.size(self.due[key]))
 
-        def share(self, ref, units=2):
-            self.go("sib", ref, units, dev(sib, x))
+        def share(self, ref, units=2, key="sib"):
+            self.go(key, ref, units, dev(sib, x))
 
         def s5(self):
             self.come("sib")
@@ -292,15 +318,15 @@
                 for half in (0, 1):
                     lo, hi = self.at(half, dp, -1), self.at(half, dp, 1)
                     if dp in (0, 1):
-                        self.go("f", lo, 2, self.q(half, 1))
+                        self.go(("f", dp), lo, 2, self.q(half, 1))
                     else:
-                        self.go("f", hi, 2, self.q(half, -1))
+                        self.go(("f", dp), hi, 2, self.q(half, -1))
                     self.share(lo)
                     self.share(hi)
 
-        def s4(self):
-            self.come("f")
-            for dp in (0, -1, 1, 2):
+        def s4(self, dps):
+            for dp in dps:
+                self.come(("f", dp))
                 for half in (0, 1):
                     self.share(self.at(half, dp, 2))
 
@@ -308,26 +334,30 @@
         def at(self, j, par, r, n):
             r = lax.rem(y + z + par, 2) * 128 + r
             cols = pl.ds(pl.multiple_of(c * 1024, 1024), 1024)
-            return ow.at[xat(j), pl.ds(pl.multiple_of(r, 32), n), cols]
+            return ow.at[POS[j % 4], pl.ds(pl.multiple_of(r, 32), n), cols]
 
         def piece(self, j, half):
             return self.at(j, 0, half * 64, 64)
+
+        def over(self, key, j, half, to):
+            d = right if to == 1 else left
+            self.go(key, self.piece(j, half), 4, d, self.piece(j - to, half))
 
         def spread(self, j, half, n):
             for i in (0, 1):
                 self.go(("y", n), self.at(j, 0, half * 64 + i * 32, 32), 2, yz(half, 1 - 2 * i))
-            self.share(self.piece(j, half), 4)
+            self.share(self.piece(j, half), 4, ("sib", n == 2))
 
         def s0(self):
-            self.go("x0", self.piece(0, 0), 4, right)
-            self.go("x0", self.piece(0, 1), 4, left)
-            self.go("x1", self.piece(0, 1), 4, right)
-            self.go("x1", self.piece(0, 0), 4, left)
+            self.over("x0", 0, 0, 1)
+            self.over("x0", 0, 1, -1)
+            self.over("x1", 0, 1, 1)
+            self.over("x1", 0, 0, -1)
 
         def s1a(self):
             self.come("x0")
-            self.go("xf", self.piece(3, 0), 4, right)
-            self.go("xf", self.piece(1, 1), 4, left)
+            self.over("xf", 3, 0, 1)
+            self.over("xf", 1, 1, -1)
             self.spread(3, 0, 0)
             self.spread(1, 1, 0)
 
@@ -344,7 +374,7 @@
         def s4(self, n):
             self.come(("y", n))
             for j, half in (((3, 0), (1, 1)), ((3, 1), (1, 0)), ((2, 0), (2, 1)))[n]:
-                self.share(self.at(j, 1, half * 64, 64), 4)
+                self.share(self.at(j, 1, half * 64, 64), 4, ("sib", n == 2))
 
     def ow_size(n):
         for quarters in (1, 2, 3, 4):
@@ -369,17 +399,18 @@
         return 0
 
     lax.fori_loop(1, 9, expand, 0)
-    phase("o1")
-    g_o.s1a()
     phase("wait_halo")
-    h_kv.wait_recv()
-    h_drow.wait_recv()
+
+    @pl.when(jnp.logical_not(first))
+    def _():
+        h_kv.wait_recv()
+        h_drow.wait_recv()
+
     phase("masks")
     expand(0, 0)
     ahead = jnp.broadcast_to(drow[7:8, :].astype(F32), (128, 128)).T
     dcol[0:HALO, :] = ahead[128 - HALO :, :]
 
-    first = sp == 0
     t_ids = lax.broadcasted_iota(jnp.int32, (ROWS, 128), 0)
     center = dcol[HALO : HALO + ROWS, :]
     ok1 = (dcol[HALO - 1 : HALO - 1 + ROWS, :] == center) & ((t_ids >= 1) | jnp.logical_not(first))
@@ -415,8 +446,11 @@
             o = o + ceil_dot(p, kvz[keys, 1024 + h * 256 : 1024 + (h + 1) * 256])
         att[pl.ds(r0, 128), :] = o.astype(BF16)
 
-    a2a = {}
-    af_col = pl.ds(pl.multiple_of(x * 256, 256), 256)
+    a2a, over, across = {}, [], []
+
+    def af_col(j):
+        return af.at[:, pl.ds(POS[(-j) % 4] * 256, 256)]
+
     for j in (2, 1, 3, 0):
         t = xat(j)
 
@@ -427,53 +461,75 @@
         phase(f"attend{j}")
         lax.fori_loop(0, 2, two, 0)
         rows = att.at[pl.ds(pl.multiple_of(t * 256, 256), 256)]
-        if j:
-            a2a[j] = push(rows, af.at[:, af_col], dev(sp, t))
+        if j == 2:
+            for h, d in ((0, right), (1, left)):
+                half = att.at[pl.ds(pl.multiple_of(t * 256 + h * 128, 128), 128)]
+                over.append(push(half, via.at[h], d))
+        elif j:
+            a2a[j] = push(rows, af_col(j), dev(sp, t))
         else:
-            l_af = local(rows, af.at[:, af_col])
+            l_af = local(rows, af_col(0))
         if j == 2:
+            phase("o1a")
+            g_o.s1a()
             phase("d0p")
             l_wd.wait()
             g_d.s0p()
         if j == 1:
             phase("o1b")
             g_o.s1b()
+        if j == 3:
+            phase("a2f")
+            for h, d in ((0, right), (1, left)):
+                over[h].wait_recv()
+                across.append(push(via.at[h], af_col(2).at[pl.ds(h * 128, 128)], d))
+            phase("u1p")
             g_u.s1p()
-        if j == 3:
-            phase("o2")
-            g_o.s2()
-            g_u.s1q(0)
+    phase("o2")
+    g_o.s2()
     phase("u1")
+    g_u.s1q(0)
     g_u.s1q(-1)
     g_u.s1q(1)
     g_o.s4(0)
     phase("a2a")
     l_af.wait()
-    for j in (1, 3, 2):
-        a2a[j].wait_recv()
+    for cp in (a2a[1], a2a[3], *across):
+        cp.wait_recv()
     phase("o4")
     g_o.s4(1)
-    g_o.s4(2)
-    phase("u2")
-    g_u.s2()
-    phase("o5")
-    g_o.s5()
-
-    phase("project")
     l_res.wait()
     l_gain.wait()
     l_cg.wait()
     l_cv.wait()
-
-    def project(j, sq):
+    phase("o5a")
+    g_o.come(("sib", False))
+
+    phase("project1")
+
+    def project1(j, _):
         col = pl.ds(pl.multiple_of(j * 512, 512), 512)
-        w = ow[:, :, col].reshape(1024, 512)
-        m = res[:, col].astype(F32) + ceil_dot(af[...], w)
+        w = ow[0:3, :, col].reshape(768, 512)
+        mid[:, col] = res[:, col].astype(F32) + ceil_dot(af[:, 0:768], w)
+        return 0
+
+    lax.fori_loop(0, D // 512, project1, 0)
+    phase("o4b")
+    g_o.s4(2)
+    phase("u2")
+    g_u.s2()
+    phase("o5b")
+    g_o.come(("sib", True))
+    phase("project2")
+
+    def project2(j, sq):
+        col = pl.ds(pl.multiple_of(j * 512, 512), 512)
+        m = mid[:, col] + ceil_dot(af[:, 768:1024], ow[3, :, col])
         m = m.astype(BF16).astype(F32)
         mid[:, col] = m
         return sq + jnp.sum(m * m, axis=-1, keepdims=True)
 
-    sq = lax.fori_loop(0, D // 512, project, jnp.zeros((BLK, 1), F32))
+    sq = lax.fori_loop(0, D // 512, project2, jnp.zeros((BLK, 1), F32))
     inv = lax.rsqrt(sq * (1.0 / D) + 1e-06)
     for h in (0, 1):
         r = slice(h * HALF, (h + 1) * HALF)
@@ -526,28 +582,26 @@
     g_d.s1p()
     phase("u3b")
     g_u.s3((-1,))
-    g_d.s1q(0)
-    g_d.s1q(-1)
     phase("u3c")
     g_u.s3((1,))
-    g_d.s1q(1)
+    g_d.s1q(0)
     phase("u3d")
     g_u.s3((2,))
+    g_d.s1q(-1)
+    g_d.s1q(1)
+    phase("d2")
+    g_d.s2()
+    phase("u4a")
+    g_u.s4((0, -1))
     phase("n_half")
     n_r0.wait_recv()
     f_r = push(rows_of(L0), rows_of(A0), right)
     n_l1.wait_recv()
     f_l = push(rows_of(R1), rows_of(A1), left)
-    phase("d2")
-    g_d.s2()
+    phase("u4c")
+    g_u.s4((1, 2))
     phase("d3a")
     g_d.s3((0,))
-    phase("u4")
-    g_u.s4()
-    phase("d3b")
-    g_d.s3((-1, 1))
-    phase("d3c")
-    g_d.s3((2,))
     phase("u5")
     g_u.s5()
     phase("tails")
@@ -563,13 +617,13 @@
     def _():
         tail0_local.wait()
 
-    def up(i):
+    def up(i, to, parts=(0, 1)):
         rows = nb[i : i + 2].reshape(PAIR, D)
-        for h in (0, 1):
+        for h in parts:
             col = pl.ds(h * HID, HID)
-            pre[:, col] = ceil_dot(rows, wu[:, col]).astype(BF16).astype(F32)
-
-    def conv(i, blocks):
+            to[:, col] = ceil_dot(rows, wu[:, col]).astype(BF16).astype(F32)
+
+    def conv(i, pre, blocks):
         def step(j, _):
             gc = pl.ds(pl.multiple_of(j * 128, 128), 128)
             vc = pl.ds(pl.multiple_of(HID + j * 128, 128), 128)
@@ -601,17 +655,23 @@
     def down(i, col):
         return nt_dot(hid[i // 2], wd[col, :])
 
-    phase("up0")
-    up(O0)
-    phase("conv0")
-    conv(O0, ((x, 0), (x, 1)))
-
     phase("up1")
-    up(R1)
-    phase("d4")
-    g_d.s4()
+    up(R1, pre)
+    phase("d3b")
+    g_d.s3((-1, 1))
+    phase("d3c")
+    g_d.s3((2,))
+    g_d.s4((0,))
     phase("conv1")
-    conv(R1, ((xat(1), 1), (xat(3), 0)))
+    conv(R1, pre, ((xat(1), 1), (xat(3), 0)))
+    phase("up0a")
+    up(O0, pre0, (0,))
+    phase("d4a")
+    g_d.s4((-1, 1))
+    phase("up0b")
+    up(O0, pre0, (1,))
+    phase("d4b")
+    g_d.s4((2,))
     phase("d5")
     g_d.s5()
     phase("down1")
@@ -622,14 +682,17 @@
         s_one.append(push(s1.at[top, col], rl.at[bot, col], right))
         s_one.append(push(s1.at[bot, col], rr.at[top, col], left))
 
+    phase("conv0")
+    conv(O0, pre0, ((x, 0), (x, 1)))
+
     phase("wait_n2")
     f_r.wait_recv()
     f_l.wait_recv()
     nb[A1, 0:HALO, :] = nb[A0, HALF:EXT, :]
     phase("up2")
-    up(A0)
+    up(A0, pre)
     phase("conv2")
-    conv(A0, ((xat(2), 0), (xat(2), 1)))
+    conv(A0, pre, ((xat(2), 0), (xat(2), 1)))
     phase("down2")
     for col in chunks:
         s2[:, col] = down(A0, col).astype(BF16)
@@ -645,9 +708,9 @@
     n_r1.wait_recv()
     nb[L1, 0:HALO, :] = nb[L0, HALF:EXT, :]
     phase("up3")
-    up(R0)
+    up(R0, pre)
     phase("conv3")
-    conv(R0, ((xat(1), 0), (xat(3), 1)))
+    conv(R0, pre, ((xat(1), 0), (xat(3), 1)))
     phase("down3")
     for col in chunks:
         p3[:, col] = down(R0, col)
@@ -679,6 +742,12 @@
     phase("wait_sends")
     for cp in copies:
         cp.wait_send()
+
+    @pl.when(jnp.logical_not(last))
+    def _():
+        h_kv.wait_send()
+        h_drow.wait_send()
+
     for g in (g_o, g_u, g_d):
         g.gone()
     phase(None)
@@ -708,7 +777,7 @@
     i32 = jnp.int32
     return pl.pallas_call(
         kernel,
-        out_shape=jax.ShapeDtypeStruct((BLK, D), BF16),
+        out_shape=pltpu.VMEM((BLK, D), BF16),
         in_specs=[any_spec] * 4 + [smem] + [any_spec] * 8,
         out_specs=pl.BlockSpec(memory_space=pltpu.VMEM),
         scratch_shapes=[
@@ -721,6 +790,7 @@
             V((ROWS, 128), F32),
             V((ROWS, 256), BF16),
             V((BLK, 1024), BF16),
+            V((2, HALF, 256), BF16),
             V((4, 256, D), BF16),
             V((BLK, D), BF16),
             V((BLK, D), F32),
@@ -728,6 +798,7 @@
             V((8, EXT, D), BF16),
             V((D, 2 * HID), BF16),
             V((D, HID), BF16),
+            V((PAIR, 2 * HID), F32),
             V((PAIR, 2 * HID), F32),
             V((4, BLK, HID), BF16),
             V((3, HID), F32),
@@ -747,7 +818,7 @@
         compiler_params=pltpu.CompilerParams(
             collective_id=0,
             has_side_effects=True,
-            vmem_limit_bytes=67_000_000,
+            vmem_limit_bytes=62_000_000,
         ),
         cost_estimate=pl.CostEstimate(
             flops=20_000_000_000, bytes_accessed=10_000_000, transcendentals=4_000_000

time: 111 us -> 104 us (0.937)
  Pallas kernels: 108 us -> 103 us
  local copies, waits for them, and re-layouts: 2.3 us -> 0.97 us
    pallas_call x1, Pallas kernels: 108 us -> 103 us  [per_device(): pl.pallas_call(kernel, out_shape=pltpu.VMEM((BLK, D), BF16), in_specs=[an...]
    unnamed x1, local copies, waits for them, and re-layouts: 2.3 us -> 0.97 us
where the time goes in v4:
time: 104 us
  Pallas kernels  103 us (99%)
    pallas_call x1, Pallas kernels, per_device(): pl.pallas_call(kernel, out_shape=pltpu.VMEM((BLK, D), BF16), in_specs=[an...  103 us

profile of v4, /device:TPU:1, one launch (start us, length us, event | category | flops | bytes accessed | tf_op | source)
XLA Modules:
  0.0 104.0 jit_solution(12551052909831885540)
XLA Ops:
  0.0 103.1 %shard_map.127 = bf16[256,2048]{1,0:T(8,128)(2,1)S(1)} custom-call(bf16[1024,256]{1,0:T(8,128)(2,1)} %q_in.1, bf16[64,1024]{1,0:T(8,128)(2,1)} %bitcast.6, bf16[64,1024]{1,0:T(8,128)(2,1)} %bitcast.7, s32[8,128]{1,0:T(8,128)} %bitcast.9, f32[4]{0:T(128)} %sinks.1, bf16[256,2048]{1,0:T(8,128)(2,1)} %res_in.1, bf16[256,2048]{1,0:T(8,128)(2,1)} %ow_in.1, ...), custom_call_target="tpu_custom_call" | custom-call | flops 20000000000 | bytes 10000000 | tf_op jit(solution)/shard_map/pallas_call | solution.py:778
  103.1 1.0 copy.15

commit v5 on v4

--- a/solution.py
+++ b/solution.py
@@ -25,7 +25,6 @@
 PAIR = 2 * EXT
 N_SEND, N_RECV = 40, 64
 R1, L0, R0, L1, O0, O1, A0, A1 = range(8)
-FIRST = {0: O0, 1: R0, 2: A0, 3: L0}
 POS = {0: 0, 1: 1, 3: 2, 2: 3}
 TN = (((0,), (0,)), ((), ()))
 
@@ -68,6 +67,7 @@
     mid,
     gain,
     nb,
+    edge,
     wu,
     wd,
     pre,
@@ -153,23 +153,6 @@
     l_cg = local(cg_in, cg)
     l_cv = local(cv_in, cv)
 
-    er = lax.broadcasted_iota(jnp.int32, (128, 2048), 0)
-    ec = lax.broadcasted_iota(jnp.int32, (128, 2048), 1)
-    sel = (
-        ((er >> 6) == (ec >> 10))
-        & ((er & 63) == (ec & 63))
-        & (((ec >> 8) & 3) == ((ec >> 6) & 3))
-    )
-    place = jnp.where(sel, 1.0, 0.0).astype(BF16)
-
-    def column(i, _):
-        r = pl.ds(pl.multiple_of(HALO + i * 128, 8), 128)
-        dcol[r, :] = jnp.broadcast_to(drow[pl.ds(8 + i, 1), :].astype(F32), (128, 128)).T
-        return 0
-
-    l_drow.wait()
-    lax.fori_loop(0, 8, column, 0)
-
     phase("barrier")
     pl.semaphore_wait(bar, 12)
 
@@ -200,6 +183,7 @@
 
     l_k.wait()
     l_v.wait()
+    l_drow.wait()
     nxt = dev(sp_next, x)
     first = sp == 0
     last = sp == N_SP - 1
@@ -301,12 +285,13 @@
                 self.go("pf", self.at(half, -1, 0, 0), 1, self.p(half, 1))
                 self.go("pf", self.at(half, 1, 0, 1), 1, self.p(half, -1))
 
-        def s1q(self, dp):
+        def s1q(self, dp, part=None):
+            n = 2 if part is None else 1
             for half in (0, 1):
-                b = self.at(half, dp, 0)
-                self.go(("q", dp), b, 2, self.q(half, 1))
-                self.go(("q", dp), b, 2, self.q(half, -1))
-                self.share(b)
+                b = self.at(half, dp, 0, part)
+                self.go(("q", dp), b, n, self.q(half, 1))
+                self.go(("q", dp), b, n, self.q(half, -1))
+                self.share(b, n)
 
         def s2(self):
             self.come("pf")
@@ -390,6 +375,23 @@
     l_wg.wait()
     l_wv.wait()
     g_u.s0p()
+
+    phase("column")
+    er = lax.broadcasted_iota(jnp.int32, (128, 2048), 0)
+    ec = lax.broadcasted_iota(jnp.int32, (128, 2048), 1)
+    sel = (
+        ((er >> 6) == (ec >> 10))
+        & ((er & 63) == (ec & 63))
+        & (((ec >> 8) & 3) == ((ec >> 6) & 3))
+    )
+    place = jnp.where(sel, 1.0, 0.0).astype(BF16)
+
+    def column(i, _):
+        r = pl.ds(pl.multiple_of(HALO + i * 128, 8), 128)
+        dcol[r, :] = jnp.broadcast_to(drow[pl.ds(8 + i, 1), :].astype(F32), (128, 128)).T
+        return 0
+
+    lax.fori_loop(0, 8, column, 0)
 
     phase("expand")
 
@@ -492,12 +494,13 @@
     g_u.s1q(-1)
     g_u.s1q(1)
     g_o.s4(0)
+    phase("o4a")
+    g_o.s4(1)
+    g_d.s1p()
     phase("a2a")
     l_af.wait()
     for cp in (a2a[1], a2a[3], *across):
         cp.wait_recv()
-    phase("o4")
-    g_o.s4(1)
     l_res.wait()
     l_gain.wait()
     l_cg.wait()
@@ -549,37 +552,23 @@
         return nb.at[i, pl.ds(0, HALO)]
 
     tail = nb.at[O1, pl.ds(HALF, HALO)]
-    t_sp = jnp.where(x == 3, sp_next, sp)
     n_mid = push(halo_of(O1), halo_of(R1), left)
-    tails = [push(tail, halo_of(FIRST[(1 - j) % 4]), dev(t_sp, xat(j))) for j in (1, 3)]
     n_r0 = push(rows_of(O0), rows_of(L0), right)
     n_l1 = push(rows_of(O1), rows_of(R1), left)
-    tails.append(push(tail, halo_of(FIRST[3]), dev(t_sp, xat(2))))
-    tail0 = pltpu.make_async_remote_copy(
-        src_ref=tail,
-        dst_ref=halo_of(R0),
-        send_sem=new("s"),
-        recv_sem=new("r"),
-        device_id=dev(sp_next, x),
-        device_id_type=MESH,
-    )
-    tail0_local = pltpu.make_async_copy(tail, halo_of(R0), loc_sem.at[len(loc)])
-    loc.append(None)
+    tails = [push(tail, halo_of(L0), dev(jnp.where(x == 3, sp_next, sp), xat(2)))]
+    edges = [remote(tail, edge, dev(sp_next, xat(j))) for j in (0, 1, 3)]
+    edge_from = {0: 3, 1: 0, 3: 2}
 
     @pl.when(x == 3)
     def _():
-        tail0.start()
-
-    @pl.when(x != 3)
-    def _():
-        tail0_local.start()
+        for cp in edges:
+            cp.start()
 
     n_r1 = push(rows_of(O1), rows_of(L1), right)
     n_l0 = push(rows_of(O0), rows_of(R0), left)
 
     phase("u3a")
     g_u.s3((0,))
-    g_d.s1p()
     phase("u3b")
     g_u.s3((-1,))
     phase("u3c")
@@ -608,14 +597,15 @@
     n_mid.wait_recv()
     for cp in tails:
         cp.wait_recv()
-
-    @pl.when(x == 3)
-    def _():
-        tail0.wait()
-
-    @pl.when(x != 3)
-    def _():
-        tail0_local.wait()
+    for j, cp in zip((0, 1, 3), edges):
+
+        @pl.when(x == edge_from[j])
+        def _(cp=cp):
+            cp.wait_recv()
+
+    def put_halo(slot, before, edge_x):
+        near = nb[before, HALF:EXT, :]
+        nb[slot, 0:HALO, :] = jnp.where(x == edge_x, edge[...], near)
 
     def up(i, to, parts=(0, 1)):
         rows = nb[i : i + 2].reshape(PAIR, D)
@@ -664,12 +654,8 @@
     g_d.s4((0,))
     phase("conv1")
     conv(R1, pre, ((xat(1), 1), (xat(3), 0)))
-    phase("up0a")
-    up(O0, pre0, (0,))
     phase("d4a")
     g_d.s4((-1, 1))
-    phase("up0b")
-    up(O0, pre0, (1,))
     phase("d4b")
     g_d.s4((2,))
     phase("d5")
@@ -682,13 +668,16 @@
         s_one.append(push(s1.at[top, col], rl.at[bot, col], right))
         s_one.append(push(s1.at[bot, col], rr.at[top, col], left))
 
-    phase("conv0")
-    conv(O0, pre0, ((x, 0), (x, 1)))
+    n_r1.wait_recv()
+    put_halo(O0, L1, 0)
+    phase("up0a")
+    up(O0, pre0, (0,))
 
     phase("wait_n2")
     f_r.wait_recv()
     f_l.wait_recv()
     nb[A1, 0:HALO, :] = nb[A0, HALF:EXT, :]
+    put_halo(A0, R1, 2)
     phase("up2")
     up(A0, pre)
     phase("conv2")
@@ -705,8 +694,8 @@
 
     phase("wait_n1")
     n_l0.wait_recv()
-    n_r1.wait_recv()
     nb[L1, 0:HALO, :] = nb[L0, HALF:EXT, :]
+    put_halo(R0, O1, 3)
     phase("up3")
     up(R0, pre)
     phase("conv3")
@@ -723,12 +712,18 @@
         s3[bot, col] = (p3[bot, col] + tr[:, col].astype(F32)).astype(BF16)
         s_three.append(push(s3.at[bot, col], rr.at[bot, col], left))
 
+    phase("wait_t0")
+    finish(0, chunks[0])
+
+    phase("up0b")
+    up(O0, pre0, (1,))
+    phase("conv0")
+    conv(O0, pre0, ((x, 0), (x, 1)))
+    phase("wait_t1")
+    finish(1, chunks[1])
     phase("down0")
     for col in chunks:
         mid[:, col] += down(O0, col)
-    for i, col in enumerate(chunks):
-        phase("wait_t")
-        finish(i, col)
 
     phase("wait_s1")
     for cp in s_one:
@@ -742,6 +737,11 @@
     phase("wait_sends")
     for cp in copies:
         cp.wait_send()
+
+    @pl.when(x == 3)
+    def _():
+        for cp in edges:
+            cp.wait_send()
 
     @pl.when(jnp.logical_not(last))
     def _():
@@ -796,6 +796,7 @@
             V((BLK, D), F32),
             V((1, D), F32),
             V((8, EXT, D), BF16),
+            V((HALO, D), BF16),
             V((D, 2 * HID), BF16),
             V((D, HID), BF16),
             V((PAIR, 2 * HID), F32),

time: 104 us -> 102 us (0.981)
  Pallas kernels: 103 us -> 101 us
    pallas_call x1, Pallas kernels: 103 us -> 101 us  [per_device(): pl.pallas_call(kernel, out_shape=pltpu.VMEM((BLK, D), BF16), in_specs=[an...]
where the time goes in v5:
time: 102 us
  Pallas kernels  101 us (99%)
    pallas_call x1, Pallas kernels, per_device(): pl.pallas_call(kernel, out_shape=pltpu.VMEM((BLK, D), BF16), in_specs=[an...  101 us

profile of v5, /device:TPU:1, one launch (start us, length us, event | category | flops | bytes accessed | tf_op | source)
XLA Modules:
  0.0 102.0 jit_solution(10075883967068667431)
XLA Ops:
  0.0 101.0 %shard_map.127 = bf16[256,2048]{1,0:T(8,128)(2,1)S(1)} custom-call(bf16[1024,256]{1,0:T(8,128)(2,1)} %q_in.1, bf16[64,1024]{1,0:T(8,128)(2,1)} %bitcast.6, bf16[64,1024]{1,0:T(8,128)(2,1)} %bitcast.7, s32[8,128]{1,0:T(8,128)} %bitcast.9, f32[4]{0:T(128)} %sinks.1, bf16[256,2048]{1,0:T(8,128)(2,1)} %res_in.1, bf16[256,2048]{1,0:T(8,128)(2,1)} %ow_in.1, ...), custom_call_target="tpu_custom_call" | custom-call | flops 20000000000 | bytes 10000000 | tf_op jit(solution)/shard_map/pallas_call | solution.py:778
  101.0 1.0 copy.15

commit v6 on v5

--- a/solution.py
+++ b/solution.py
@@ -236,6 +236,7 @@
             self.sent = 0
             self.sem = {}
             self.due = {}
+            self.held = []
 
         def go(self, key, ref, units, d, dst=None):
             if key not in self.sem:
@@ -291,11 +292,18 @@
                 b = self.at(half, dp, 0, part)
                 self.go(("q", dp), b, n, self.q(half, 1))
                 self.go(("q", dp), b, n, self.q(half, -1))
+                self.held.append((b, n))
+
+        def hand_over(self):
+            for b, n in self.held:
                 self.share(b, n)
+            self.held = []
 
         def s2(self):
             self.come("pf")
             self.s1q(2)
+            if self is not g_u:
+                self.hand_over()
 
         def s3(self, dps):
             for dp in dps:
@@ -375,6 +383,8 @@
     l_wg.wait()
     l_wv.wait()
     g_u.s0p()
+    l_wd.wait()
+    g_d.s0p()
 
     phase("column")
     er = lax.broadcasted_iota(jnp.int32, (128, 2048), 0)
@@ -460,6 +470,9 @@
             attend(t * 2 + i)
             return 0
 
+        if j == 0:
+            phase("o2")
+            g_o.s2()
         phase(f"attend{j}")
         lax.fori_loop(0, 2, two, 0)
         rows = att.at[pl.ds(pl.multiple_of(t * 256, 256), 256)]
@@ -475,22 +488,19 @@
             phase("o1a")
             g_o.s1a()
             phase("d0p")
-            l_wd.wait()
-            g_d.s0p()
+            g_u.s1q(0, 0)
         if j == 1:
             phase("o1b")
             g_o.s1b()
+            phase("u1p")
+            g_u.s1p()
         if j == 3:
             phase("a2f")
             for h, d in ((0, right), (1, left)):
                 over[h].wait_recv()
                 across.append(push(via.at[h], af_col(2).at[pl.ds(h * 128, 128)], d))
-            phase("u1p")
-            g_u.s1p()
-    phase("o2")
-    g_o.s2()
     phase("u1")
-    g_u.s1q(0)
+    g_u.s1q(0, 1)
     g_u.s1q(-1)
     g_u.s1q(1)
     g_o.s4(0)
@@ -567,6 +577,7 @@
     n_r1 = push(rows_of(O1), rows_of(L1), right)
     n_l0 = push(rows_of(O0), rows_of(R0), left)
 
+    g_u.hand_over()
     phase("u3a")
     g_u.s3((0,))
     phase("u3b")
@@ -646,9 +657,13 @@
         return nt_dot(hid[i // 2], wd[col, :])
 
     phase("up1")
-    up(R1, pre)
+    up(R1, pre, (0,))
     phase("d3b")
-    g_d.s3((-1, 1))
+    g_d.s3((-1,))
+    phase("up1b")
+    up(R1, pre, (1,))
+    phase("d3b2")
+    g_d.s3((1,))
     phase("d3c")
     g_d.s3((2,))
     g_d.s4((0,))

time: 102 us -> 102 us (level)
  no operation moved by 1% of the time
where the time goes in v6:
time: 102 us
  Pallas kernels  101 us (99%)
    pallas_call x1, Pallas kernels, per_device(): pl.pallas_call(kernel, out_shape=pltpu.VMEM((BLK, D), BF16), in_specs=[an...  101 us

profile of v6, /device:TPU:1, one launch (start us, length us, event | category | flops | bytes accessed | tf_op | source)
XLA Modules:
  0.0 101.9 jit_solution(13619889376320278924)
XLA Ops:
  0.0 101.0 %shard_map.127 = bf16[256,2048]{1,0:T(8,128)(2,1)S(1)} custom-call(bf16[1024,256]{1,0:T(8,128)(2,1)} %q_in.1, bf16[64,1024]{1,0:T(8,128)(2,1)} %bitcast.6, bf16[64,1024]{1,0:T(8,128)(2,1)} %bitcast.7, s32[8,128]{1,0:T(8,128)} %bitcast.9, f32[4]{0:T(128)} %sinks.1, bf16[256,2048]{1,0:T(8,128)(2,1)} %res_in.1, bf16[256,2048]{1,0:T(8,128)(2,1)} %ow_in.1, ...), custom_call_target="tpu_custom_call" | custom-call | flops 20000000000 | bytes 10000000 | tf_op jit(solution)/shard_map/pallas_call | solution.py:793
  101.0 1.0 copy.15

commit v7 on v5

--- a/solution.py
+++ b/solution.py
@@ -534,6 +534,12 @@
 
     sq = lax.fori_loop(0, D // 512, project2, jnp.zeros((BLK, 1), F32))
     inv = lax.rsqrt(sq * (1.0 / D) + 1e-06)
+    def rows_of(i):
+        return nb.at[i, pl.ds(HALO, HALF)]
+
+    def halo_of(i):
+        return nb.at[i, pl.ds(0, HALO)]
+
     for h in (0, 1):
         r = slice(h * HALF, (h + 1) * HALF)
         for j in range(D // 512):
@@ -542,19 +548,14 @@
             nb[O0 + h, HALO:EXT, col] = n
             if h == 0:
                 nb[O1, 0:HALO, col] = n[HALF - HALO :]
+        if h == 0:
+            n_r0 = push(rows_of(O0), rows_of(L0), right)
 
     phase("send_n")
 
-    def rows_of(i):
-        return nb.at[i, pl.ds(HALO, HALF)]
-
-    def halo_of(i):
-        return nb.at[i, pl.ds(0, HALO)]
-
     tail = nb.at[O1, pl.ds(HALF, HALO)]
+    n_l1 = push(rows_of(O1), rows_of(R1), left)
     n_mid = push(halo_of(O1), halo_of(R1), left)
-    n_r0 = push(rows_of(O0), rows_of(L0), right)
-    n_l1 = push(rows_of(O1), rows_of(R1), left)
     tails = [push(tail, halo_of(L0), dev(jnp.where(x == 3, sp_next, sp), xat(2)))]
     edges = [remote(tail, edge, dev(sp_next, xat(j))) for j in (0, 1, 3)]
     edge_from = {0: 3, 1: 0, 3: 2}

time: 102 us -> 102 us (level)
  no operation moved by 1% of the time
where the time goes in v7:
time: 102 us
  Pallas kernels  101 us (99%)
    pallas_call x1, Pallas kernels, per_device(): pl.pallas_call(kernel, out_shape=pltpu.VMEM((BLK, D), BF16), in_specs=[an...  101 us

profile of v7, /device:TPU:1, one launch (start us, length us, event | category | flops | bytes accessed | tf_op | source)
XLA Modules:
  0.0 101.8 jit_solution(6646043781922146989)
XLA Ops:
  0.0 100.8 %shard_map.127 = bf16[256,2048]{1,0:T(8,128)(2,1)S(1)} custom-call(bf16[1024,256]{1,0:T(8,128)(2,1)} %q_in.1, bf16[64,1024]{1,0:T(8,128)(2,1)} %bitcast.6, bf16[64,1024]{1,0:T(8,128)(2,1)} %bitcast.7, s32[8,128]{1,0:T(8,128)} %bitcast.9, f32[4]{0:T(128)} %sinks.1, bf16[256,2048]{1,0:T(8,128)(2,1)} %res_in.1, bf16[256,2048]{1,0:T(8,128)(2,1)} %ow_in.1, ...), custom_call_target="tpu_custom_call" | custom-call | flops 20000000000 | bytes 10000000 | tf_op jit(solution)/shard_map/pallas_call | solution.py:779
  100.8 1.0 copy.15
